TPU v7x, 512 devices: a whole 4x4x16 slice. The times are simulated.
512 devices in a mesh: ep: 32 (over z, core), tp: 16 (over y, x).
Axes of the slice: x: 4, y: 4, z: 16, core: 2. Of those that a mesh axis runs over, the one named last changes fastest.
Arguments:
- queries: bfloat16 [12288, 2048], P('ep', 'tp'), may hold values from -6 to 6
- keys: bfloat16 [12288, 2048], P('ep', 'tp'), may hold values from -6 to 6
- values: bfloat16 [12288, 2048], P('ep', 'tp'), may hold values from -6 to 6
- key_bias: bfloat16 [12288, 16], P('ep', 'tp'), may hold values from -14 to -1.5
- moe_in: bfloat16 [4096, 2048], P(('ep', 'tp')), may hold values from -6 to 6
- norm_gain: float32 [2048], replicated, may hold values from 0.1 to 1.9
- route_ids: int32 [4096, 4], P('ep'), may hold values from 0 to 63, all different within a row; in each aligned block of 8 rows (0 to 7, 8 to 15, ...) at most 1 rows name the same one
- route_weights: float32 [4096, 4], P(('ep', 'tp')), may hold values from 0.1 to 1
- gate_weight: bfloat16 [64, 1024, 2048], P('ep', 'tp'), may hold values from -0.125 to 0.125
- up_weight: bfloat16 [64, 1024, 2048], P('ep', 'tp'), may hold values from -0.125 to 0.125
- down_weight: bfloat16 [64, 1024, 2048], P('ep', 'tp'), may hold values from -0.1875 to 0.1875
- shared_gate: bfloat16 [1024, 2048], P('tp'), may hold values from -0.125 to 0.125
- shared_up: bfloat16 [1024, 2048], P('tp'), may hold values from -0.125 to 0.125
- shared_down: bfloat16 [1024, 2048], P('tp'), may hold values from -0.1875 to 0.1875
Outputs:
- heads_out: bfloat16 [12288, 2048], P('ep', 'tp')
- moe_out: bfloat16 [4096, 2048], P(('ep', 'tp'))
Inputs may be any that keep to these rules, and one draw needn't show every extreme that they name: `route_ids`: each row names 4 different experts. Among the 8 rows of one device (an aligned block of 8 rows) no expert is named more than once.
All inputs are finite; a program needn't handle non-finite values.
Results may differ from a plain program's by a relative error of at most 0.015.
Values may be sent and summed in bfloat16 or wider, within the bound.
A program may use at most 128 MiB of HBM per device.

v0:
```python
import jax
import jax.numpy as jnp
from jax import lax
from jax.sharding import Mesh
from jax.sharding import PartitionSpec as P

TP = ("tp_0", "tp_1")
EP_TP = ("ep", "tp_0", "tp_1")


norm_eps = 1e-05


def in_one_piece(arrays, axis, dim, along):
    widths = [a.shape[along] for a in arrays]
    both = jnp.concatenate(arrays, axis=along)
    filled = lax.all_gather(both, axis, axis=dim, tiled=True)
    return tuple(jnp.split(filled, [sum(widths[:k]) for k in range(1, len(widths))], axis=along))


def joined_along(pieces, dim):
    pieces = jnp.moveaxis(pieces, 0, dim)
    lengths = pieces.shape
    return pieces.reshape(*lengths[:dim], lengths[dim] * lengths[dim + 1], *lengths[dim + 2 :])


def from_everyone(value, axis):
    copies = jnp.broadcast_to(value, (lax.axis_size(axis), *value.shape))
    return lax.all_to_all(copies, axis, split_axis=0, concat_axis=0, tiled=True)


def gather_directly(value, axis, dim):
    return joined_along(from_everyone(value, axis), dim)


def summed_rows(terms, axes):
    so_far = terms.astype(jnp.bfloat16)
    for axis in axes:
        so_far = lax.psum_scatter(so_far, axis, scatter_dimension=0, tiled=True)
    return so_far.astype(jnp.float32)


def stick_half(queries, keys, values, key_bias):
    num_rows, width = queries.shape
    local_heads = key_bias.shape[1]
    head_dim = width // local_heads
    all_keys, all_values, all_bias = in_one_piece((keys, values, key_bias), "ep", 0, 1)
    total = all_keys.shape[0]
    kblock = min(1024, total)
    first_row = lax.axis_index("ep") * num_rows
    query_pos = first_row + jnp.arange(num_rows, dtype=jnp.int32)
    top_block = (first_row + num_rows - 1) // kblock
    q_heads = queries.reshape(num_rows, local_heads, head_dim)
    scale_factor = head_dim ** (-0.5)

    def visit(count, carried):
        accum, later = carried
        offset = (top_block - count) * kblock
        k_block = lax.dynamic_slice_in_dim(all_keys, offset, kblock, 0).reshape(
            kblock, local_heads, head_dim
        )
        v_block = lax.dynamic_slice_in_dim(all_values, offset, kblock, 0).reshape(
            kblock, local_heads, head_dim
        )
        b_block = lax.dynamic_slice_in_dim(all_bias, offset, kblock, 0).astype(jnp.float32)
        scores = (
            jnp.einsum("qhd,khd->hqk", q_heads, k_block, preferred_element_type=jnp.float32)
            * scale_factor
        )
        scores = scores + b_block.T[:, None, :]
        key_pos = offset + jnp.arange(kblock, dtype=jnp.int32)
        causal = key_pos[None, :] < query_pos[:, None]
        log_keep = jnp.where(causal, -jax.nn.softplus(scores), 0.0)
        between = lax.cumsum(log_keep, axis=2, reverse=True) - log_keep + later[:, :, None]
        weights = jnp.where(causal, jnp.exp(jax.nn.log_sigmoid(scores) + between), 0.0).astype(
            jnp.bfloat16
        )
        accum = accum + jnp.einsum(
            "hqk,khd->hqd", weights, v_block, preferred_element_type=jnp.float32
        )
        return (accum, later + jnp.sum(log_keep, axis=2))

    initial = (
        jnp.zeros((local_heads, num_rows, head_dim), jnp.float32),
        jnp.zeros((local_heads, num_rows), jnp.float32),
    )
    raw_out, _ = lax.fori_loop(0, top_block + 1, visit, initial)
    scaled = raw_out * lax.rsqrt(jnp.mean(raw_out * raw_out, axis=2, keepdims=True) + norm_eps)
    return jnp.transpose(scaled, (1, 0, 2)).reshape(num_rows, width).astype(jnp.bfloat16)


def expert_terms(
    routed, shared_rows, gate_weight, up_weight, down_weight, shared_gate, shared_up, shared_down
):
    blocks = routed.shape[0]
    width = routed.shape[3]
    gate_val = jnp.einsum("besd,efd->besf", routed, gate_weight, preferred_element_type=jnp.float32)
    up_val = jnp.einsum("besd,efd->besf", routed, up_weight, preferred_element_type=jnp.float32)
    hidden = (jax.nn.silu(gate_val) * up_val).astype(jnp.bfloat16)
    routed_out = jnp.einsum(
        "besf,efd->besd", hidden, down_weight, preferred_element_type=jnp.float32
    )
    routed_out = routed_out.reshape(blocks, -1, width)
    shared_gv = jnp.einsum(
        "nd,fd->nf", shared_rows, shared_gate, preferred_element_type=jnp.float32
    )
    shared_uv = jnp.einsum("nd,fd->nf", shared_rows, shared_up, preferred_element_type=jnp.float32)
    shared_hidden = (jax.nn.silu(shared_gv) * shared_uv).astype(jnp.bfloat16)
    shared_out = jnp.einsum(
        "nf,fd->nd", shared_hidden, shared_down, preferred_element_type=jnp.float32
    )
    shared_out = shared_out.reshape(blocks, -1, width)
    return jnp.concatenate([routed_out, shared_out], axis=1).reshape(-1, width)


def expert_half(
    moe_in,
    norm_gain,
    route_ids,
    route_weights,
    gate_weight,
    up_weight,
    down_weight,
    shared_gate,
    shared_up,
    shared_down,
):
    own_rows, width = moe_in.shape
    top_k = route_weights.shape[1]
    local_experts = gate_weight.shape[0]
    ep_count = lax.axis_size("ep")
    tp_count = lax.axis_size(TP)
    expert_count = local_experts * ep_count
    capacity = max(1, 2 * own_rows * tp_count * top_k // (tp_count * expert_count))
    slot_total = local_experts * ep_count * capacity
    term_rows = slot_total + own_rows
    tp_index = lax.axis_index(TP)
    as_float = moe_in.astype(jnp.float32)
    normed = (
        as_float
        * lax.rsqrt(jnp.mean(as_float * as_float, axis=1, keepdims=True) + norm_eps)
        * norm_gain
    ).astype(jnp.bfloat16)
    flat_ids = route_ids.reshape(tp_count, own_rows * top_k)
    one_hot = (flat_ids[:, :, None] == jnp.arange(expert_count, dtype=jnp.int32)).astype(jnp.int32)
    ranks = jnp.sum((jnp.cumsum(one_hot, axis=1) - one_hot) * one_hot, axis=2)
    dest_ep = flat_ids // local_experts
    local_index = flat_ids % local_experts
    local_slot = local_index * (ep_count * capacity) + dest_ep * capacity + ranks
    own_slots = lax.dynamic_index_in_dim(local_slot, tp_index, 0, keepdims=False)
    row_of = jnp.arange(own_rows * top_k, dtype=jnp.int32) // top_k
    source_row = jnp.full((slot_total,), own_rows, jnp.int32).at[own_slots].set(row_of)
    outgoing = jnp.take(normed, source_row, axis=0, mode="fill", fill_value=0)
    outgoing = outgoing.reshape(local_experts, ep_count, capacity, width)
    arrived = lax.all_to_all(outgoing, "ep", split_axis=1, concat_axis=1, tiled=True)
    pooled = gather_directly(
        jnp.concatenate([arrived.reshape(slot_total, width), normed], axis=0), TP, 0
    )
    blocks = term_rows * lax.axis_size(TP) // term_rows
    portion = pooled.reshape(blocks, term_rows, width)
    routed = portion[:, :slot_total].reshape(blocks, local_experts, ep_count * capacity, width)
    shared_rows = portion[:, slot_total:].reshape(blocks * own_rows, width)
    summed = summed_rows(
        expert_terms(
            routed,
            shared_rows,
            gate_weight,
            up_weight,
            down_weight,
            shared_gate,
            shared_up,
            shared_down,
        ),
        TP,
    )
    slot_out = (
        summed[:slot_total].astype(jnp.bfloat16).reshape(local_experts, ep_count, capacity, width)
    )
    returned = lax.all_to_all(slot_out, "ep", split_axis=1, concat_axis=1, tiled=True).reshape(
        slot_total, width
    )
    picked = (
        jnp.take(returned, own_slots, axis=0).astype(jnp.float32).reshape(own_rows, top_k, width)
    )
    combined = summed[slot_total:] + jnp.sum(picked * route_weights[:, :, None], axis=1)
    return combined.astype(jnp.bfloat16)


def shards(
    queries,
    keys,
    values,
    key_bias,
    moe_in,
    norm_gain,
    route_ids,
    route_weights,
    gate_weight,
    up_weight,
    down_weight,
    shared_gate,
    shared_up,
    shared_down,
):
    heads_out = stick_half(queries, keys, values, key_bias)
    moe_out = expert_half(
        moe_in,
        norm_gain,
        route_ids,
        route_weights,
        gate_weight,
        up_weight,
        down_weight,
        shared_gate,
        shared_up,
        shared_down,
    )
    return (heads_out, moe_out)


def solution(mesh):
    split = Mesh(mesh.devices.reshape(mesh.shape["ep"], 4, 4), ("ep", "tp_0", "tp_1"))
    return jax.shard_map(
        shards,
        mesh=split,
        in_specs=(
            P("ep", TP),
            P("ep", TP),
            P("ep", TP),
            P("ep", TP),
            P(EP_TP, None),
            P(),
            P("ep", None),
            P(EP_TP, None),
            P("ep", TP, None),
            P("ep", TP, None),
            P("ep", TP, None),
            P(TP, None),
            P(TP, None),
            P(TP, None),
        ),
        out_specs=(P("ep", TP), P(EP_TP, None)),
        check_vma=False,
    )
```

profile of v0, /device:TPU:481, one launch (start us, length us, event | category | flops | bytes accessed | tf_op | source)
XLA Modules:
  0.0 401.9 jit_solution(17209294233976188353)
XLA Ops:
  9.0 1.7 pad_maximum_fusion.1
  16.5 28.3 %all_to_all.15 = bf16[2,32,1,2048]{3,0,2,1:T(2,128)(2,1)S(1)} all-to-all(bf16[2,32,1,2048]{3,0,2,1:T(2,128)(2,1)S(1)} %broadcast_select_fusion), channel_id=1, replica_groups=mesh['ep'=32,'tp_0'=4,'tp_1'=4] {'ep'}, dimensions={1} | all-to-all | bytes 524288 | tf_op jit(solution)/shard_map/all_to_all | solution.py:155
  45.6 61.7 %all_to_all.16 = bf16[16,72,2048]{2,1,0:T(8,128)(2,1)S(1)} all-to-all(bf16[16,72,2048]{2,1,0:T(8,128)(2,1)S(1)} %broadcast_in_dim.58), channel_id=1, replica_groups=mesh['ep'=32,'tp_0'=4,'tp_1'=4] {'tp_0','tp_1'}, dimensions={0} | all-to-all | bytes 9437184 | tf_op jit(solution)/shard_map/all_to_all | solution.py:29
  107.9 1.6 copy-done.1
  109.5 1.9 copy-done.2
  112.7 6.5 %convert_bitcast_fusion = bf16[16,2,32,2048]{3,2,0,1:T(8,128)(2,1)} fusion(bf16[16,2,32,2048]{3,2,1,0:T(8,128)(2,1)} %bitcast.128, bf16[2,64,2048]{2,1,0:T(8,128)(2,1)S(1)} %copy-done, bf16[2,64,2048]{2,1,0:T(8,128)(2,1)S(1)} %copy-done.7, f32[16,2,32,64]{3,2,0,1:T(8,128)S(1)} %fusion.27), kind=kOutput, calls=%fused_computation.41 | convolution fusion | flops 539361280 | bytes 9699328 | tf_op jit(solution)/shard_map/besf,efd->besd/dot_general | solution.py:100
  119.3 4.8 %copy.63 = bf16[16,2,32,2048]{3,2,1,0:T(8,128)(2,1)} copy(bf16[16,2,32,2048]{3,2,0,1:T(8,128)(2,1)} %convert_bitcast_fusion) | data formatting | bytes 8388608 | tf_op jit(solution)/shard_map/besf,efd->besd/transpose | solution.py:100
  125.4 1.9 fusion.26
  127.3 5.1 %pad_maximum_fusion = bf16[16,72,2048]{2,1,0:T(8,128)(2,1)} fusion(bf16[16,8,2048]{2,1,0:T(8,128)(2,1)S(1)} %fusion.26, bf16[16,64,2048]{2,1,0:T(8,128)(2,1)} %bitcast.125), kind=kLoop, calls=%fused_computation.40 | loop fusion | flops 9437184 | bytes 9437184 | tf_op jit(solution)/shard_map/concatenate | solution.py:113
  133.2 3.2 split.13
  136.4 3.2 copy.51
  139.6 47.8 %reduce-scatter.3.cloned.1.call-done = bf16[288,2048]{1,0:T(8,128)(2,1)} async-done(((bf16[1152,2048]{1,0:T(8,128)(2,1)}), bf16[288,2048]{1,0:T(8,128)(2,1)}) %reduce-scatter.3.cloned.1.call-update) | async-done | bytes 1179664 | tf_op jit(solution)/shard_map/reduce_scatter | solution.py:39
  187.4 4.8 %fusion.78 = (bf16[12288,128]{1,0:T(8,128)(2,1)}, bf16[12288,128]{1,0:T(8,128)(2,1)}) fusion(bf16[12288,257]{1,0:T(8,128)(2,1)} %all-gather.2.cloned.1.call-done), kind=kLoop, calls=%fused_computation.121 | loop fusion | bytes 12582912 | tf_op jit(solution)/shard_map/split | solution.py:18
  192.2 28.0 %reduce-scatter.5.cloned.1.call-done = bf16[72,2048]{1,0:T(8,128)(2,1)} async-done(((bf16[288,2048]{1,0:T(8,128)(2,1)}), bf16[72,2048]{1,0:T(8,128)(2,1)}) %reduce-scatter.5.cloned.1.call-update) | async-done | bytes 294928 | tf_op jit(solution)/shard_map/reduce_scatter | solution.py:39
  222.1 13.7 %all-to-all-start.2 = ((bf16[2,32,1,2048]{3,0,2,1:T(2,128)(2,1)}), bf16[2,32,1,2048]{3,0,2,1:T(2,128)(2,1)S(1)}, u32[]{:S(2)}, u32[]{:S(2)}) async-start(bf16[2,32,1,2048]{3,0,2,1:T(2,128)(2,1)} %copy.64), calls=%async_computation.4 | async-start | bytes 524288 | tf_op jit(solution)/shard_map/all_to_all | solution.py:179
  235.8 155.3 %while.13 = (s32[]{:T(128)}, f32[1,384,128]{2,1,0:T(8,128)S(1)}, f32[1,384]{1,0:T(1,128)S(1)}, s32[]{:T(128)}, s32[]{:T(128)}, /*index=5*/bf16[12288,128]{1,0:T(...) while((s32[]{:T(128)}, f32[1,384,128]{2,1,0:T(8,128)S(1)}, ...), condition=%wide.region_4.5_spmd.clone, body=%wide.region_0.4_spmd.clone.sunk | while | flops 265103360 | bytes 15295711 | solution.py:87
  236.1 3.4 fusion.94
  239.5 3.8 fusion.95
  243.6 3.9 fusion.96
  247.5 1.4 fusion.97
  249.0 3.4 fusion.94
  252.4 3.8 fusion.95
  256.6 3.9 fusion.96
  260.5 1.4 fusion.97
  261.9 3.4 fusion.94
  265.3 3.8 fusion.95
  269.5 3.9 fusion.96
  274.8 3.4 fusion.94
  278.2 3.8 fusion.95
  282.4 3.9 fusion.96
  286.3 1.4 fusion.97
  287.8 3.4 fusion.94
  291.2 3.8 fusion.95
  295.3 3.9 fusion.96
  299.2 1.4 fusion.97
  300.7 3.4 fusion.94
  304.1 3.8 fusion.95
  308.3 3.9 fusion.96
  312.2 1.4 fusion.97
  313.6 3.4 fusion.94
  317.0 3.8 fusion.95
  321.2 3.9 fusion.96
  325.1 1.4 fusion.97
  326.6 3.4 fusion.94
  329.9 3.8 fusion.95
  334.1 3.9 fusion.96
  338.0 1.4 fusion.97
  339.5 3.4 fusion.94
  342.9 3.8 fusion.95
  347.0 3.9 fusion.96
  350.9 1.4 fusion.97
  352.4 3.4 fusion.94
  355.8 3.8 fusion.95
  360.0 3.9 fusion.96
  363.9 1.4 fusion.97
  365.3 3.4 fusion.94
  368.7 3.8 fusion.95
  372.9 3.9 fusion.96
  376.8 1.4 fusion.97
  378.3 3.4 fusion.94
  381.7 3.8 fusion.95
  385.8 3.9 fusion.96
  389.7 1.4 fusion.97
  393.1 1.4 add_convert_fusion
  (165 shorter events, 21.4 us)
Async XLA Ops:
  8.0 104.7 %copy-start = (bf16[2,64,2048]{2,1,0:T(8,128)(2,1)S(1)}, bf16[2,64,2048]{2,1,0:T(8,128)(2,1)}, u32[]{:S(2)}) copy-start(bf16[2,64,2048]{2,1,0:T(8,128)(2,1)} %param.26) | copy-start | bytes 1572868
  8.0 125.2 %all-gather.2.cloned.1.call-start = ((), (), s32[]{:S(2)}) async-start(), calls=%async_computation.5 | async-start | bytes 9732096 | tf_op jit(solution)/shard_map/all_gather | solution.py:17
  10.7 176.7 %reduce-scatter.3.cloned.1.call-start = ((), (), s32[]{:S(2)}) async-start(), calls=%async_computation.6 | async-start | bytes 5898240 | tf_op jit(solution)/shard_map/reduce_scatter | solution.py:39
  107.3 2.2 copy-start.1
  107.3 4.2 %copy-start.6 = (bf16[2,64,2048]{2,1,0:T(8,128)(2,1)S(1)}, bf16[2,64,2048]{2,1,0:T(8,128)(2,1)}, u32[]{:S(2)}) copy-start(bf16[2,64,2048]{2,1,0:T(8,128)(2,1)} %param.24) | copy-start | bytes 1572868
  109.5 1.9 copy-start.2
  111.5 1.3 copy-start.7
  119.2 4.8 %copy-start.8 = (bf16[64,2048]{1,0:T(8,128)(2,1)S(1)}, bf16[64,2048]{1,0:T(8,128)(2,1)}, u32[]{:S(2)}) copy-start(bf16[64,2048]{1,0:T(8,128)(2,1)} %param.27) | copy-start | bytes 786436
  119.2 6.1 %copy-start.3 = (bf16[64,2048]{1,0:T(8,128)(2,1)S(1)}, bf16[64,2048]{1,0:T(8,128)(2,1)}, u32[]{:S(2)}) copy-start(bf16[64,2048]{1,0:T(8,128)(2,1)} %param.29) | copy-start | bytes 786436
  119.2 6.2 %copy-start.4 = (bf16[64,2048]{1,0:T(8,128)(2,1)S(1)}, bf16[64,2048]{1,0:T(8,128)(2,1)}, u32[]{:S(2)}) copy-start(bf16[64,2048]{1,0:T(8,128)(2,1)} %param.28) | copy-start | bytes 786436
  132.4 0.7 copy-start.5
  132.5 87.7 %reduce-scatter.5.cloned.1.call-start = ((), (), s32[]{:S(2)}) async-start(), calls=%async_computation.7 | async-start | bytes 1474560 | tf_op jit(solution)/shard_map/reduce_scatter | solution.py:39
  192.2 43.6 %copy-start.9 = (bf16[384,128]{1,0:T(8,128)(2,1)S(1)}, bf16[384,128]{1,0:T(8,128)(2,1)}, u32[]{:S(2)}) copy-start(bf16[384,128]{1,0:T(8,128)(2,1)} %param.16) | copy-start | bytes 294916
  222.1 170.0 %all-to-all-start.2 = ((bf16[2,32,1,2048]{3,0,2,1:T(2,128)(2,1)}), bf16[2,32,1,2048]{3,0,2,1:T(2,128)(2,1)S(1)}, u32[]{:S(2)}, u32[]{:S(2)}) async-start(bf16[2,32,1,2048]{3,0,2,1:T(2,128)(2,1)} %copy.64), calls=%async_computation.4 | async-start | bytes 524288 | tf_op jit(solution)/shard_map/all_to_all | solution.py:179
Sparse Core Ops, SparseCore 0:
  10.9 87.8 all-gather.1
Sparse Core Ops, SparseCore 1:
  132.5 54.8 reduce-scatter.2
  190.1 30.0 reduce-scatter.4
where the time goes:
time: 404 us; the launch traced here: 402 us
  other arithmetic  106 us (26%)
  blocking collectives  90 us (22%)
  waiting for transfers between devices  75.8 us (19%)
  matrix products  68.2 us (17%)
  local copies, waits for them, and re-layouts  31.5 us (8%)
  between operations  15.7 us (4%)
  starting transfers between devices  13.8 us (3%)
    reduce_scatter x2, waiting for transfers between devices, summed_rows(): so_far = lax.psum_scatter(so_far, axis, scatter_dimension=0, tiled=True)  75.7 us
    all_to_all x1, blocking collectives, from_everyone(): return lax.all_to_all(copies, axis, split_axis=0, concat_axis=0, tiled=True)  61.7 us
    convert_element_type x12, other arithmetic, visit(): jnp.where(causal, jnp.exp(jax.nn.log_sigmoid(scores) + between), 0.0)  46.7 us
    another operation x24, other arithmetic  45.7 us
    dot_general x12, matrix products, visit(): jnp.einsum('qhd,khd->hqk', q_heads, k_block, preferred_element_type=jnp.f...  40.7 us
    all_to_all x1, blocking collectives, expert_half(): lax.all_to_all(outgoing, 'ep', split_axis=1, concat_axis=1, tiled=True)  28.3 us
    dot_general x12, matrix products, visit(): jnp.einsum('hqk,khd->hqd', weights, v_block, preferred_element_type=jnp.f...  16.5 us
    all_to_all x1, starting transfers between devices, expert_half(): lax.all_to_all(slot_out, 'ep', split_axis=1, concat_axis=1, tiled=True)  13.7 us
  transfers between devices with their start and end apart: 4, of which 2 were waited for; matrix products, arithmetic and copies ran while one was open for 48% of the time, Pallas kernels for 0%

commit v1 on v0

--- a/solution.py
+++ b/solution.py
@@ -1,6 +1,10 @@
+import functools
+
 import jax
 import jax.numpy as jnp
 from jax import lax
+from jax.experimental import pallas as pl
+from jax.experimental.pallas import tpu as pltpu
 from jax.sharding import Mesh
 from jax.sharding import PartitionSpec as P
 
@@ -40,53 +44,94 @@
     return so_far.astype(jnp.float32)
 
 
+def packed_rows(keys, values, key_bias):
+    num_rows, width = keys.shape
+    bias_rows = key_bias.reshape(num_rows // width, width)
+    return jnp.concatenate(
+        [keys, values, jnp.pad(bias_rows, ((0, 16 - bias_rows.shape[0]), (0, 0)))], axis=0
+    )
+
+
+def attention_kernel(scale_factor, q_ref, kv_ref, o_ref, tri, acc, later):
+    num_rows, width = q_ref.shape
+    chunk = 128
+    me = lax.axis_index("ep")
+    row_id = lax.broadcasted_iota(jnp.int32, (num_rows, num_rows + 128), 0)
+    col_id = lax.broadcasted_iota(jnp.int32, (num_rows, num_rows + 128), 1)
+    tri[...] = jnp.where((row_id > col_id) | (col_id >= num_rows), -1.0, 0.0).astype(jnp.bfloat16)
+    acc[...] = jnp.zeros_like(acc)
+    later[...] = jnp.zeros_like(later)
+
+    def visit(block, diagonal):
+        k_block = kv_ref[block, :num_rows, :]
+        v_block = kv_ref[block, num_rows : 2 * num_rows, :]
+        bias = kv_ref[block, 2 * num_rows : 2 * num_rows + 16, :].astype(jnp.float32)
+        bias = jnp.concatenate([bias[r : r + 1] for r in range(num_rows // width)], axis=1)
+        for first in range(0, num_rows, chunk):
+            rows = slice(first, first + chunk)
+            scores = (
+                lax.dot_general(
+                    q_ref[rows, :],
+                    k_block,
+                    (((1,), (1,)), ((), ())),
+                    preferred_element_type=jnp.float32,
+                )
+                * scale_factor
+                + bias
+            )
+            soft = jnp.maximum(scores, jnp.log(1.0 + jnp.exp(jnp.minimum(scores, 88.0))))
+            dropped = soft
+            if diagonal:
+                causal = lax.broadcasted_iota(
+                    jnp.int32, scores.shape, 1
+                ) < first + lax.broadcasted_iota(jnp.int32, scores.shape, 0)
+                dropped = jnp.where(causal, soft, 0.0)
+            sums = jnp.dot(
+                dropped.astype(jnp.bfloat16), tri[...], preferred_element_type=jnp.float32
+            )
+            carried = later[rows, :]
+            between = sums[:, :num_rows] + jnp.concatenate(
+                [carried] * (num_rows // width), axis=1
+            )
+            weights = jnp.exp(scores - soft + between)
+            if diagonal:
+                weights = jnp.where(causal, weights, 0.0)
+            acc[rows, :] += jnp.dot(
+                weights.astype(jnp.bfloat16), v_block, preferred_element_type=jnp.float32
+            )
+            later[rows, :] = carried + sums[:, num_rows:]
+
+    visit(me, True)
+
+    def earlier(count, carry):
+        visit(me - 1 - count, False)
+        return carry
+
+    lax.fori_loop(0, me, earlier, 0)
+    raw_out = acc[...]
+    o_ref[...] = (
+        raw_out * lax.rsqrt(jnp.mean(raw_out * raw_out, axis=1, keepdims=True) + norm_eps)
+    ).astype(jnp.bfloat16)
+
+
 def stick_half(queries, keys, values, key_bias):
     num_rows, width = queries.shape
-    local_heads = key_bias.shape[1]
-    head_dim = width // local_heads
-    all_keys, all_values, all_bias = in_one_piece((keys, values, key_bias), "ep", 0, 1)
-    total = all_keys.shape[0]
-    kblock = min(1024, total)
-    first_row = lax.axis_index("ep") * num_rows
-    query_pos = first_row + jnp.arange(num_rows, dtype=jnp.int32)
-    top_block = (first_row + num_rows - 1) // kblock
-    q_heads = queries.reshape(num_rows, local_heads, head_dim)
-    scale_factor = head_dim ** (-0.5)
-
-    def visit(count, carried):
-        accum, later = carried
-        offset = (top_block - count) * kblock
-        k_block = lax.dynamic_slice_in_dim(all_keys, offset, kblock, 0).reshape(
-            kblock, local_heads, head_dim
-        )
-        v_block = lax.dynamic_slice_in_dim(all_values, offset, kblock, 0).reshape(
-            kblock, local_heads, head_dim
-        )
-        b_block = lax.dynamic_slice_in_dim(all_bias, offset, kblock, 0).astype(jnp.float32)
-        scores = (
-            jnp.einsum("qhd,khd->hqk", q_heads, k_block, preferred_element_type=jnp.float32)
-            * scale_factor
-        )
-        scores = scores + b_block.T[:, None, :]
-        key_pos = offset + jnp.arange(kblock, dtype=jnp.int32)
-        causal = key_pos[None, :] < query_pos[:, None]
-        log_keep = jnp.where(causal, -jax.nn.softplus(scores), 0.0)
-        between = lax.cumsum(log_keep, axis=2, reverse=True) - log_keep + later[:, :, None]
-        weights = jnp.where(causal, jnp.exp(jax.nn.log_sigmoid(scores) + between), 0.0).astype(
-            jnp.bfloat16
-        )
-        accum = accum + jnp.einsum(
-            "hqk,khd->hqd", weights, v_block, preferred_element_type=jnp.float32
-        )
-        return (accum, later + jnp.sum(log_keep, axis=2))
-
-    initial = (
-        jnp.zeros((local_heads, num_rows, head_dim), jnp.float32),
-        jnp.zeros((local_heads, num_rows), jnp.float32),
-    )
-    raw_out, _ = lax.fori_loop(0, top_block + 1, visit, initial)
-    scaled = raw_out * lax.rsqrt(jnp.mean(raw_out * raw_out, axis=2, keepdims=True) + norm_eps)
-    return jnp.transpose(scaled, (1, 0, 2)).reshape(num_rows, width).astype(jnp.bfloat16)
+    filled = lax.all_gather(packed_rows(keys, values, key_bias), "ep", axis=0, tiled=False)
+    return pl.pallas_call(
+        functools.partial(attention_kernel, width ** (-0.5)),
+        out_shape=jax.ShapeDtypeStruct((num_rows, width), jnp.bfloat16),
+        in_specs=[pl.BlockSpec(memory_space=pltpu.VMEM)] * 2,
+        out_specs=pl.BlockSpec(memory_space=pltpu.VMEM),
+        scratch_shapes=[
+            pltpu.VMEM((num_rows, num_rows + 128), jnp.bfloat16),
+            pltpu.VMEM((num_rows, width), jnp.float32),
+            pltpu.VMEM((num_rows, 128), jnp.float32),
+        ],
+        compiler_params=pltpu.CompilerParams(vmem_limit_bytes=40 * 1024 * 1024),
+        cost_estimate=pl.CostEstimate(
+            flops=8_000_000_000, bytes_accessed=7_000_000, transcendentals=14_000_000
+        ),
+    )(queries, filled)
 
 
 def expert_terms(

time: 404 us -> 327 us (0.81)
  other arithmetic: 106 us -> 10.6 us
  matrix products: 68.2 us -> 11 us
  waiting for transfers between devices: 75.8 us -> 127 us
  Pallas kernels: 0 us -> 42.5 us
  local copies, waits for them, and re-layouts: 31.5 us -> 18.6 us
    dot_general x24 -> x0, matrix products: 57.3 us -> none  [the longest x12 40.7 us: visit(): jnp.einsum('qhd,khd->hqk', q_heads, k_block, preferred_element_type=jnp.f...]
    convert_element_type x13 -> x0, other arithmetic: 47.5 us -> none  [the longest x12 46.7 us: visit(): jnp.where(causal, jnp.exp(jax.nn.log_sigmoid(scores) + between), 0.0)]
    another operation x24 -> x0, other arithmetic: 45.7 us -> none
    pallas_call x0 -> x1, Pallas kernels: none -> 42.5 us  [stick_half(): pl.pallas_call(functools.partial(attention_kernel, width ** (-0.5)), out_...]
    all_gather x1, waiting for transfers between devices: 0.02 us -> 37.9 us  [stick_half(): lax.all_gather(packed_rows(keys, values, key_bias), 'ep', axis=0, tiled=F...]
    reduce_scatter x2, waiting for transfers between devices: 75.7 us -> 88.6 us  [summed_rows(): so_far = lax.psum_scatter(so_far, axis, scatter_dimension=0, tiled=True)]
    split x2 -> x0, local copies, waits for them, and re-layouts: 7.93 us -> none  [in_one_piece(): jnp.split(filled, [sum(widths[:k]) for k in range(1, len(widths))], axis=...]
    unnamed x24 -> x30, local copies, waits for them, and re-layouts: 9.12 us -> 7.91 us
  transfers between devices with their start and end apart: 4 -> 4, of which waited for: 2 -> 3; matrix products, arithmetic and copies ran while one was open for 48% -> 1% of each run, Pallas kernels for 0% -> 13%
where the time goes in v1:
time: 327 us; the launch traced here: 326 us
  waiting for transfers between devices  127 us (39%)
  blocking collectives  87.4 us (27%)
  Pallas kernels  42.5 us (13%)
  local copies, waits for them, and re-layouts  18.6 us (6%)
  between operations  15.7 us (5%)
  starting transfers between devices  13.6 us (4%)
  matrix products  11 us (3%)
  other arithmetic  10.6 us (3%)
    reduce_scatter x2, waiting for transfers between devices, summed_rows(): so_far = lax.psum_scatter(so_far, axis, scatter_dimension=0, tiled=True)  88.6 us
    all_to_all x1, blocking collectives, from_everyone(): return lax.all_to_all(copies, axis, split_axis=0, concat_axis=0, tiled=True)  62.5 us
    pallas_call x1, Pallas kernels, stick_half(): pl.pallas_call(functools.partial(attention_kernel, width ** (-0.5)), out_...  42.5 us
    all_gather x1, waiting for transfers between devices, stick_half(): lax.all_gather(packed_rows(keys, values, key_bias), 'ep', axis=0, tiled=F...  37.9 us
    all_to_all x1, blocking collectives, expert_half(): lax.all_to_all(outgoing, 'ep', split_axis=1, concat_axis=1, tiled=True)  24.9 us
    all_to_all x1, starting transfers between devices, expert_half(): lax.all_to_all(slot_out, 'ep', split_axis=1, concat_axis=1, tiled=True)  13.5 us
    unnamed x30, local copies, waits for them, and re-layouts  7.91 us
  transfers between devices with their start and end apart: 4, of which 3 were waited for; matrix products, arithmetic and copies ran while one was open for 1% of the time, Pallas kernels for 13%

profile of v1, /device:TPU:481, one launch (start us, length us, event | category | flops | bytes accessed | tf_op | source)
XLA Modules:
  0.0 326.0 jit_solution(1170852826468536114)
XLA Ops:
  8.0 0.0 copy-start
  8.0 0.0 reduce-scatter.3.cloned.1.call-start
  8.1 0.8 copy.36
  8.9 0.1 reshape.111
  9.0 0.1 copy.37
  9.1 0.8 fusion.57
  9.9 0.2 fusion.47
  10.2 0.7 scatter_custom_fusion
  10.9 0.9 fusion.36
  11.8 0.1 broadcast_in_dim.36
  11.9 0.1 copy.42
  12.0 0.8 fusion.38
  12.8 0.7 gather_fusion
  13.6 0.3 broadcast_select_fusion
  13.9 24.9 %all_to_all.15 = bf16[2,32,1,2048]{3,0,2,1:T(2,128)(2,1)S(1)} all-to-all(bf16[2,32,1,2048]{3,0,2,1:T(2,128)(2,1)S(1)} %broadcast_select_fusion), channel_id=1, replica_groups=mesh['ep'=32,'tp_0'=4,'tp_1'=4] {'ep'}, dimensions={1} | all-to-all | bytes 524288 | tf_op jit(solution)/shard_map/all_to_all | solution.py:200
  38.8 0.1 copy.44
  38.9 0.6 broadcast_in_dim.40
  39.5 62.5 %all_to_all.16 = bf16[16,72,2048]{2,1,0:T(8,128)(2,1)S(1)} all-to-all(bf16[16,72,2048]{2,1,0:T(8,128)(2,1)S(1)} %broadcast_in_dim.40), channel_id=1, replica_groups=mesh['ep'=32,'tp_0'=4,'tp_1'=4] {'tp_0','tp_1'}, dimensions={0} | all-to-all | bytes 9437184 | tf_op jit(solution)/shard_map/all_to_all | solution.py:33
  102.0 0.0 copy-start.3
  102.0 2.1 copy-done.3
  104.1 0.6 slice.25
  104.7 0.0 copy-start.4
  104.7 0.0 copy-start.12
  104.7 2.0 copy-done.4
  106.7 0.0 copy-done.11
  106.7 1.2 fusion.5
  107.9 0.0 copy-done
  108.0 0.0 copy-done.12
  108.0 6.5 %convert_bitcast_fusion = bf16[16,2,32,2048]{3,2,0,1:T(8,128)(2,1)} fusion(bf16[16,2,32,2048]{3,2,1,0:T(8,128)(2,1)} %bitcast.56, bf16[2,64,2048]{2,1,0:T(8,128)(2,1)S(1)} %copy-done, bf16[2,64,2048]{2,1,0:T(8,128)(2,1)S(1)} %copy-done.12, f32[16,2,32,64]{3,2,0,1:T(8,128)S(1)} %fusion.5), kind=kOutput, calls=%fused_computation.4 | convolution fusion | flops 539361280 | bytes 9699328 | tf_op jit(solution)/shard_map/besf,efd->besd/dot_general | solution.py:145
  114.5 4.9 %copy.47 = bf16[16,2,32,2048]{3,2,1,0:T(8,128)(2,1)} copy(bf16[16,2,32,2048]{3,2,0,1:T(8,128)(2,1)} %convert_bitcast_fusion) | data formatting | bytes 8388608 | tf_op jit(solution)/shard_map/besf,efd->besd/transpose | solution.py:145
  119.4 0.0 copy-done.13
  119.4 1.3 fusion.30
  120.7 0.0 copy-done.5
  120.7 0.0 copy-done.6
  120.7 1.9 fusion.4
  122.6 5.0 %pad_maximum_fusion = bf16[16,72,2048]{2,1,0:T(8,128)(2,1)} fusion(bf16[16,8,2048]{2,1,0:T(8,128)(2,1)S(1)} %fusion.4, bf16[16,64,2048]{2,1,0:T(8,128)(2,1)} %bitcast.53), kind=kLoop, calls=%fused_computation.3 | loop fusion | flops 9437184 | bytes 9437184 | tf_op jit(solution)/shard_map/concatenate | solution.py:158
  127.6 0.0 copy-start.2
  127.7 0.0 reduce-scatter.3.cloned.1.call-update
  127.7 0.0 reduce-scatter.5.cloned.1.call-start
  127.7 56.5 %reduce-scatter.3.cloned.1.call-done = bf16[288,2048]{1,0:T(8,128)(2,1)} async-done(((bf16[1152,2048]{1,0:T(8,128)(2,1)}), bf16[288,2048]{1,0:T(8,128)(2,1)}) %reduce-scatter.3.cloned.1.call-update) | async-done | bytes 1179664 | tf_op jit(solution)/shard_map/reduce_scatter | solution.py:43
  184.2 0.0 reduce-scatter.5.cloned.1.call-update
  184.2 0.0 all-gather.3.cloned.1.call-start
  184.3 0.0 copy-done.10
  184.3 0.0 copy-done.7
  184.3 0.0 copy-done.8
  184.3 0.7 fusion.34
  185.0 0.0 all-gather.3.cloned.1.call-update
  185.1 32.1 %reduce-scatter.5.cloned.1.call-done = bf16[72,2048]{1,0:T(8,128)(2,1)} async-done(((bf16[288,2048]{1,0:T(8,128)(2,1)}), bf16[72,2048]{1,0:T(8,128)(2,1)}) %reduce-scatter.5.cloned.1.call-update) | async-done | bytes 294928 | tf_op jit(solution)/shard_map/reduce_scatter | solution.py:43
  217.2 1.0 slice.28
  218.2 1.0 copy.48
  219.1 13.5 %all-to-all-start.2 = ((bf16[2,32,1,2048]{3,0,2,1:T(2,128)(2,1)}), bf16[2,32,1,2048]{3,0,2,1:T(2,128)(2,1)S(1)}, u32[]{:S(2)}, u32[]{:S(2)}) async-start(bf16[2,32,1,2048]{3,0,2,1:T(2,128)(2,1)} %copy.48), calls=%async_computation.4 | async-start | bytes 524288 | tf_op jit(solution)/shard_map/all_to_all | solution.py:224
  232.7 0.1 squeeze.7
  232.8 0.0 copy-done.9
  232.8 0.1 copy.50
  232.8 37.9 %all-gather.3.cloned.1.call-done = bf16[25088,128]{1,0:T(8,128)(2,1)} async-done(((bf16[784,128]{1,0:T(8,128)(2,1)}), bf16[25088,128]{1,0:T(8,128)(2,1)}) %all-gather.3.cloned.1.call-update) | async-done | bytes 6422544 | tf_op jit(solution)/shard_map/all_gather | solution.py:119
  270.7 0.0 copy-done.2
  270.7 2.8 copy-done.1
  273.6 42.5 %shard_map.149 = bf16[384,128]{1,0:T(8,128)(2,1)} custom-call(bf16[384,128]{1,0:T(8,128)(2,1)S(1)} %copy-done.2, bf16[32,784,128]{2,1,0:T(8,128)(2,1)S(1)} %bitcast.51), custom_call_target="tpu_custom_call" | custom-call | flops 8000000000 | bytes 7000000 | tf_op jit(solution)/shard_map/pallas_call | solution.py:120
  316.1 0.0 all-to-all-done.2
  316.1 0.1 copy.49
  316.2 0.7 gather_fusion.1
  316.8 0.1 gather.15
  316.9 0.3 multiply_reduce_fusion
  317.2 1.4 add_convert_fusion
  (21 shorter events, 0.1 us)
Async XLA Ops:
  8.0 99.9 %copy-start = (bf16[2,64,2048]{2,1,0:T(8,128)(2,1)S(1)}, bf16[2,64,2048]{2,1,0:T(8,128)(2,1)}, u32[]{:S(2)}) copy-start(bf16[2,64,2048]{2,1,0:T(8,128)(2,1)} %param.24) | copy-start | bytes 1572868
  8.0 176.2 %reduce-scatter.3.cloned.1.call-start = ((), (), s32[]{:S(2)}) async-start(), calls=%async_computation.5 | async-start | bytes 5898240 | tf_op jit(solution)/shard_map/reduce_scatter | solution.py:43
  102.0 2.1 copy-start.3
  104.1 2.6 copy-start.11
  104.7 2.0 copy-start.4
  104.7 3.3 copy-start.12
  114.5 4.9 %copy-start.13 = (bf16[64,2048]{1,0:T(8,128)(2,1)S(1)}, bf16[64,2048]{1,0:T(8,128)(2,1)}, u32[]{:S(2)}) copy-start(bf16[64,2048]{1,0:T(8,128)(2,1)} %param.25) | copy-start | bytes 786436
  114.5 6.2 %copy-start.5 = (bf16[64,2048]{1,0:T(8,128)(2,1)S(1)}, bf16[64,2048]{1,0:T(8,128)(2,1)}, u32[]{:S(2)}) copy-start(bf16[64,2048]{1,0:T(8,128)(2,1)} %param.27) | copy-start | bytes 786436
  114.5 6.2 %copy-start.6 = (bf16[64,2048]{1,0:T(8,128)(2,1)S(1)}, bf16[64,2048]{1,0:T(8,128)(2,1)}, u32[]{:S(2)}) copy-start(bf16[64,2048]{1,0:T(8,128)(2,1)} %param.26) | copy-start | bytes 786436
  127.6 56.7 %copy-start.10 = (bf16[384,1]{0,1:T(2,128)(2,1)S(1)}, bf16[384,1]{0,1:T(2,128)(2,1)}, u32[]{:S(2)}) copy-start(bf16[384,1]{0,1:T(2,128)(2,1)} %param.17) | copy-start | bytes 2308
  127.6 56.7 %copy-start.7 = (bf16[384,128]{1,0:T(8,128)(2,1)S(1)}, bf16[384,128]{1,0:T(8,128)(2,1)}, u32[]{:S(2)}) copy-start(bf16[384,128]{1,0:T(8,128)(2,1)} %param.16) | copy-start | bytes 294916
  127.6 56.7 %copy-start.8 = (bf16[384,128]{1,0:T(8,128)(2,1)S(1)}, bf16[384,128]{1,0:T(8,128)(2,1)}, u32[]{:S(2)}) copy-start(bf16[384,128]{1,0:T(8,128)(2,1)} %param.15) | copy-start | bytes 294916
  127.6 105.1 %copy-start.9 = (f32[8,4]{0,1:T(4,128)S(1)}, f32[8,4]{0,1:T(4,128)}, u32[]{:S(2)}) copy-start(f32[8,4]{0,1:T(4,128)} %param.21) | copy-start | bytes 388
  127.6 143.1 %copy-start.2 = (bf16[384,128]{1,0:T(8,128)(2,1)S(1)}, bf16[384,128]{1,0:T(8,128)(2,1)}, u32[]{:S(2)}) copy-start(bf16[384,128]{1,0:T(8,128)(2,1)} %q_ref.1) | copy-start | bytes 294916
  127.7 89.5 %reduce-scatter.5.cloned.1.call-start = ((), (), s32[]{:S(2)}) async-start(), calls=%async_computation.6 | async-start | bytes 1474560 | tf_op jit(solution)/shard_map/reduce_scatter | solution.py:43
  184.2 86.5 %all-gather.3.cloned.1.call-start = ((), (), s32[]{:S(2)}) async-start(), calls=%async_computation.7 | async-start | bytes 6623232 | tf_op jit(solution)/shard_map/all_gather | solution.py:119
  219.1 97.0 %all-to-all-start.2 = ((bf16[2,32,1,2048]{3,0,2,1:T(2,128)(2,1)}), bf16[2,32,1,2048]{3,0,2,1:T(2,128)(2,1)S(1)}, u32[]{:S(2)}, u32[]{:S(2)}) async-start(bf16[2,32,1,2048]{3,0,2,1:T(2,128)(2,1)} %copy.48), calls=%async_computation.4 | async-start | bytes 524288 | tf_op jit(solution)/shard_map/all_to_all | solution.py:224
  270.7 2.8 copy-start.1
Sparse Core Ops, SparseCore 0:
  127.8 56.3 reduce-scatter.2
  187.1 30.0 reduce-scatter.4
Sparse Core Ops, SparseCore 1:
  186.8 83.8 all-gather.2

commit v2 on v1

v2 whole, which is shorter than its diff:
```python
import functools

import jax
import jax.numpy as jnp
from jax import lax
from jax.experimental import pallas as pl
from jax.experimental.pallas import tpu as pltpu
from jax.sharding import Mesh
from jax.sharding import PartitionSpec as P

TP = ("tp_0", "tp_1")
EP_TP = ("ep", "tp_0", "tp_1")


norm_eps = 1e-05
MESH = pl.DeviceIdType.MESH


def packed_rows(keys, values, key_bias):
    num_rows, width = keys.shape
    bias_rows = key_bias.reshape(num_rows // width, width)
    return jnp.concatenate(
        [keys, values, jnp.pad(bias_rows, ((0, 16 - bias_rows.shape[0]), (0, 0)))], axis=0
    )


def attention_kernel(scale_factor, q_ref, kv_ref, o_ref, tri, acc, later):
    num_rows, width = q_ref.shape
    chunk = 128
    me = lax.axis_index("ep")
    row_id = lax.broadcasted_iota(jnp.int32, (num_rows, num_rows + 128), 0)
    col_id = lax.broadcasted_iota(jnp.int32, (num_rows, num_rows + 128), 1)
    tri[...] = jnp.where((row_id > col_id) | (col_id >= num_rows), -1.0, 0.0).astype(jnp.bfloat16)
    acc[...] = jnp.zeros_like(acc)
    later[...] = jnp.zeros_like(later)

    def visit(block, diagonal):
        k_block = kv_ref[block, :num_rows, :]
        v_block = kv_ref[block, num_rows : 2 * num_rows, :]
        bias = kv_ref[block, 2 * num_rows : 2 * num_rows + 16, :].astype(jnp.float32)
        bias = jnp.concatenate([bias[r : r + 1] for r in range(num_rows // width)], axis=1)
        for first in range(0, num_rows, chunk):
            rows = slice(first, first + chunk)
            scores = (
                lax.dot_general(
                    q_ref[rows, :],
                    k_block,
                    (((1,), (1,)), ((), ())),
                    preferred_element_type=jnp.float32,
                )
                * scale_factor
                + bias
            )
            soft = jnp.maximum(scores, jnp.log(1.0 + jnp.exp(jnp.minimum(scores, 88.0))))
            dropped = soft
            if diagonal:
                causal = lax.broadcasted_iota(
                    jnp.int32, scores.shape, 1
                ) < first + lax.broadcasted_iota(jnp.int32, scores.shape, 0)
                dropped = jnp.where(causal, soft, 0.0)
            sums = jnp.dot(
                dropped.astype(jnp.bfloat16), tri[...], preferred_element_type=jnp.float32
            )
            carried = later[rows, :]
            between = sums[:, :num_rows] + jnp.concatenate(
                [carried] * (num_rows // width), axis=1
            )
            weights = jnp.exp(scores - soft + between)
            if diagonal:
                weights = jnp.where(causal, weights, 0.0)
            acc[rows, :] += jnp.dot(
                weights.astype(jnp.bfloat16), v_block, preferred_element_type=jnp.float32
            )
            later[rows, :] = carried + sums[:, num_rows:]

    visit(me, True)

    def earlier(count, carry):
        visit(me - 1 - count, False)
        return carry

    lax.fori_loop(0, me, earlier, 0)
    raw_out = acc[...]
    o_ref[...] = (
        raw_out * lax.rsqrt(jnp.mean(raw_out * raw_out, axis=1, keepdims=True) + norm_eps)
    ).astype(jnp.bfloat16)


def stick_half(queries, keys, values, key_bias):
    num_rows, width = queries.shape
    filled = lax.all_gather(packed_rows(keys, values, key_bias), "ep", axis=0, tiled=False)
    return pl.pallas_call(
        functools.partial(attention_kernel, width ** (-0.5)),
        out_shape=jax.ShapeDtypeStruct((num_rows, width), jnp.bfloat16),
        in_specs=[pl.BlockSpec(memory_space=pltpu.VMEM)] * 2,
        out_specs=pl.BlockSpec(memory_space=pltpu.VMEM),
        scratch_shapes=[
            pltpu.VMEM((num_rows, num_rows + 128), jnp.bfloat16),
            pltpu.VMEM((num_rows, width), jnp.float32),
            pltpu.VMEM((num_rows, 128), jnp.float32),
        ],
        compiler_params=pltpu.CompilerParams(vmem_limit_bytes=40 * 1024 * 1024),
        cost_estimate=pl.CostEstimate(
            flops=8_000_000_000, bytes_accessed=7_000_000, transcendentals=14_000_000
        ),
    )(queries, filled)


def expert_kernel(
    moe_in,
    gain,
    ids,
    ids_across,
    mix,
    gate,
    up,
    down,
    shared_gate,
    shared_up,
    shared_down,
    out,
    w_in,
    w_out,
    w_shared,
    cut,
    mixes,
    pre,
    outgoing,
    pooled,
    partial,
    inbox,
    result,
    shared_sum,
    returned,
    comb,
    cut_back,
    landed,
    w_sem,
    pre_send,
    pre_recv,
    mix_send,
    mix_recv,
    go_send,
    go_recv,
    ag_send,
    ag_recv,
    rs_send,
    rs_recv,
    back_send,
    back_recv,
    fin_send,
    fin_recv,
):
    ep_count, tp_count = lax.axis_size("ep"), 16
    rows = moe_in.shape[0]
    e = lax.axis_index("ep")
    y = lax.axis_index("tp_0")
    x = lax.axis_index("tp_1")
    t = y * 4 + x

    def tp_peer(k):
        other = lax.rem(t + k, tp_count)
        return other, {"tp_0": other // 4, "tp_1": lax.rem(other, 4)}

    barrier = pltpu.get_barrier_semaphore()

    def greet_tp(k, carry):
        pl.semaphore_signal(barrier, inc=1, device_id=tp_peer(k)[1], device_id_type=MESH)
        return carry

    def greet_ep(k, carry):
        pl.semaphore_signal(
            barrier, inc=1, device_id={"ep": lax.rem(e + k, ep_count)}, device_id_type=MESH
        )
        return carry

    lax.fori_loop(1, ep_count, greet_ep, 0)
    lax.fori_loop(1, tp_count, greet_tp, 0)

    loads = [
        pltpu.make_async_copy(gate, w_in.at[pl.ds(0, 2)], w_sem.at[0]),
        pltpu.make_async_copy(up, w_in.at[pl.ds(2, 2)], w_sem.at[1]),
        pltpu.make_async_copy(down, w_out, w_sem.at[2]),
        pltpu.make_async_copy(shared_gate, w_shared.at[0], w_sem.at[3]),
        pltpu.make_async_copy(shared_up, w_shared.at[1], w_sem.at[4]),
        pltpu.make_async_copy(shared_down, w_shared.at[2], w_sem.at[5]),
    ]
    for load in loads:
        load.start()

    as_float = moe_in[...].astype(jnp.float32)
    normed = (
        as_float
        * lax.rsqrt(jnp.mean(as_float * as_float, axis=1, keepdims=True) + norm_eps)
        * gain[...]
    ).astype(jnp.bfloat16)
    for k in range(tp_count):
        cut[k] = normed[:, k * 128 : (k + 1) * 128]
    own_ids = ids[pl.ds(pl.multiple_of(t * rows, rows), rows), :]
    own_mix = mix[...]
    lane = lax.broadcasted_iota(jnp.int32, (rows, 128), 1)
    spread = jnp.zeros((rows, 128), jnp.float32)
    for k in range(mix.shape[1]):
        spread = spread + jnp.where(own_ids[:, k : k + 1] == lane, own_mix[:, k : k + 1], 0.0)
    mixes[t] = spread
    pre[t] = cut[t]

    pl.semaphore_wait(barrier, ep_count + tp_count - 2)

    def send_pre(k, carry):
        other, device = tp_peer(k)
        pltpu.make_async_remote_copy(
            cut.at[other], pre.at[t], pre_send, pre_recv, device_id=device, device_id_type=MESH
        ).start()
        return carry

    def send_mix(k, carry):
        _, device = tp_peer(k)
        pltpu.make_async_remote_copy(
            mixes.at[t], mixes.at[t], mix_send, mix_recv, device_id=device, device_id_type=MESH
        ).start()
        return carry

    lax.fori_loop(1, tp_count, send_pre, 0)
    lax.fori_loop(1, tp_count, send_mix, 0)

    across = ids_across[...]
    expert_id = lax.broadcasted_iota(jnp.int32, (64, 128), 0)
    named = across[0:1] == expert_id
    for k in range(1, across.shape[0]):
        named = named | (across[k : k + 1] == expert_id)
    named = named.astype(jnp.float32)
    source = lax.broadcasted_iota(jnp.int32, (tp_count, 128), 0)
    same = (lax.broadcasted_iota(jnp.int32, (tp_count, 128), 1) // rows == source).astype(
        jnp.float32
    )
    for k in range(64):
        outgoing[k * 16 : (k + 1) * 16, :] = (same * named[k : k + 1, :]).astype(jnp.bfloat16)

    pltpu.make_async_copy(
        pre.at[pl.ds(0, tp_count - 1)], pre.at[pl.ds(0, tp_count - 1)], pre_recv
    ).wait()
    own_rows = pre[...].astype(jnp.float32).reshape(tp_count * rows, 128).astype(jnp.bfloat16)
    pooled[t, 1024:1152, :] = own_rows
    for k in range(4):
        part = slice(k * 256, (k + 1) * 256)
        outgoing[part, :] = jnp.dot(
            outgoing[part, :], own_rows, preferred_element_type=jnp.float32
        ).astype(jnp.bfloat16)
    at_e = pl.ds(pl.multiple_of(e * 32, 32), 32)

    def send_go(k, carry):
        other = lax.rem(e + k, ep_count)
        pltpu.make_async_remote_copy(
            outgoing.at[pl.ds(pl.multiple_of(other * 32, 32), 32)],
            pooled.at[t, at_e],
            go_send,
            go_recv,
            device_id={"ep": other},
            device_id_type=MESH,
        ).start()
        return carry

    lax.fori_loop(1, ep_count, send_go, 0)
    pooled[t, at_e, :] = outgoing[at_e, :]

    pltpu.make_async_copy(
        mixes.at[pl.ds(0, tp_count - 1)], mixes.at[pl.ds(0, tp_count - 1)], mix_recv
    ).wait()
    mix_all = mixes[...].reshape(tp_count * rows, 128)
    high = mix_all.astype(jnp.bfloat16)
    low = (mix_all - high.astype(jnp.float32)).astype(jnp.bfloat16)
    for k in range(4):
        column = k * 256 + lax.broadcasted_iota(jnp.int32, (128, 256), 1)
        row = lax.broadcasted_iota(jnp.int32, (128, 256), 0)
        widen = (column // 16 == row).astype(jnp.bfloat16)
        keep = lax.rem(column, 16) == row // rows
        for part, value in ((0, high), (1, low)):
            wide = jnp.dot(value, widen, preferred_element_type=jnp.float32)
            comb[part, :, k * 256 : (k + 1) * 256] = jnp.where(keep, wide, 0.0).astype(
                jnp.bfloat16
            )

    pltpu.make_async_copy(
        pooled.at[t, pl.ds(0, 992)], pooled.at[t, pl.ds(0, 992)], go_recv
    ).wait()

    quarter = 288
    names = ("tp_0", "tp_1")
    place = {"tp_0": y, "tp_1": x}

    def axes(q):
        first, second = names if q < 2 else names[::-1]
        return first, second, 1 if q % 2 == 0 else 3

    def index_at(q, df, dg):
        first, second, _ = axes(q)
        moved = {
            first: lax.rem(place[first] + df % 4, 4),
            second: lax.rem(place[second] + dg % 4, 4),
        }
        return moved["tp_0"] * 4 + moved["tp_1"]

    def block(ref, q, df, dg):
        return ref.at[index_at(q, df, dg), pl.ds(q * quarter, quarter)]

    def ag_copy(q, df, dg, along_first, step):
        first, second, _ = axes(q)
        axis = first if along_first else second
        there = ((df - step) % 4, dg % 4) if along_first else (df % 4, (dg - step) % 4)
        ref = block(pooled, q, df, dg)
        return pltpu.make_async_remote_copy(
            ref,
            ref,
            ag_send,
            ag_recv.at[q, there[0] * 4 + there[1]],
            device_id={axis: lax.rem(place[axis] + step % 4, 4)},
            device_id_type=MESH,
        )

    def ag_wait(q, df, dg):
        ref = block(pooled, q, df, dg)
        pltpu.make_async_copy(ref, ref, ag_recv.at[q, (df % 4) * 4 + dg % 4]).wait()

    quarters = range(4)
    for q in quarters:
        ag_copy(q, 0, 0, True, 1).start()
        ag_copy(q, 0, 0, True, 3).start()
    for q in quarters:
        ag_copy(q, 0, 0, False, 1).start()
        ag_copy(q, 0, 0, False, 3).start()
    for q in quarters:
        d = axes(q)[2]
        ag_wait(q, -d, 0)
        ag_copy(q, -d, 0, True, d).start()
        ag_copy(q, -d, 0, False, 1).start()
        ag_copy(q, -d, 0, False, 3).start()
    for q in quarters:
        d = axes(q)[2]
        ag_wait(q, d, 0)
        ag_copy(q, d, 0, False, 1).start()
        ag_copy(q, d, 0, False, 3).start()
    for q in quarters:
        d = axes(q)[2]
        ag_wait(q, 0, -d)
        ag_copy(q, 0, -d, False, d).start()
    for q in quarters:
        ag_wait(q, 2, 0)
        ag_copy(q, 2, 0, False, 1).start()
        ag_copy(q, 2, 0, False, 3).start()
    for hop in range(3):
        for q in quarters:
            d = axes(q)[2]
            df = (-d, d, 2)[hop]
            ag_wait(q, df, -d)
            ag_copy(q, df, -d, False, d).start()

    for load in loads:
        load.wait()

    def rs_copy(q, ref, slot, along_first, step):
        first, second, _ = axes(q)
        axis = first if along_first else second
        return pltpu.make_async_remote_copy(
            ref,
            inbox.at[q, slot],
            rs_send,
            rs_recv.at[q, slot],
            device_id={axis: lax.rem(place[axis] + step % 4, 4)},
            device_id_type=MESH,
        )

    def rs_wait(q, slot):
        ref = inbox.at[q, slot]
        pltpu.make_async_copy(ref, ref, rs_recv.at[q, slot]).wait()

    def plus(q, df, dg, *slots):
        where = index_at(q, df, dg)
        total = partial[where, q * quarter : (q + 1) * quarter, :].astype(jnp.float32)
        for slot in slots:
            total = total + inbox[q, slot].astype(jnp.float32)
        return where, total

    def silu_times(both):
        half = both.shape[1] // 2
        gate_val = both[:, :half]
        return gate_val * (1.0 / (1.0 + jnp.exp(-gate_val))) * both[:, half:]

    def feed(span, weights_in, weights_out, routed):
        both = jnp.concatenate([pooled[k, span, :] for k in range(tp_count)], axis=1)
        hidden = silu_times(
            lax.dot_general(
                both, weights_in, (((1,), (1,)), ((), ())), preferred_element_type=jnp.float32
            )
        )
        if routed:
            row = lax.broadcasted_iota(jnp.int32, hidden.shape, 0)
            column = lax.broadcasted_iota(jnp.int32, hidden.shape, 1)
            hidden = jnp.where(lax.rem(row // 16, 2) == column // 64, hidden, 0.0)
        hidden = hidden.astype(jnp.bfloat16)
        for k in range(0, tp_count, 2):
            term = jnp.dot(
                hidden,
                weights_out[:, k * 128 : (k + 2) * 128],
                preferred_element_type=jnp.float32,
            ).astype(jnp.bfloat16)
            partial[k, span, :] = term[:, :128]
            partial[k + 1, span, :] = term[:, 128:]

    for q in quarters:
        d = axes(q)[2]
        for df in range(4):
            ag_wait(q, df, d)
            ag_wait(q, df, 2)
        last = q == 3
        span = slice(q * quarter, 1024 if last else (q + 1) * quarter)
        feed(span, w_in[...].reshape(256, 2048), w_out[...].reshape(128, 2048), True)
        if last:
            feed(
                slice(1024, 1152), w_shared[0:2].reshape(128, 2048), w_shared[2], False
            )
        for df in (2, -d, d, 0):
            slot = (df % 4) * 3
            rs_copy(q, block(partial, q, df, 2), slot, False, d).start()
            rs_copy(q, block(partial, q, df, -d), slot + 1, False, -d).start()

    rows_of = lambda q: slice(q * quarter, (q + 1) * quarter)
    for turn in range(4):
        for q in quarters:
            d = axes(q)[2]
            df = (2, -d, d, 0)[turn] % 4
            rs_wait(q, df * 3)
            where, total = plus(q, df, d, df * 3)
            partial[where, rows_of(q), :] = total.astype(jnp.bfloat16)
            rs_copy(q, block(partial, q, df, d), df * 3 + 2, False, d).start()
    for turn in range(4):
        for q in quarters:
            d = axes(q)[2]
            df = (2, -d, d, 0)[turn] % 4
            rs_wait(q, df * 3 + 1)
            rs_wait(q, df * 3 + 2)
            slots = [df * 3 + 1, df * 3 + 2]
            if turn == 2:
                rs_wait(q, 12)
                slots.append(12)
            where, total = plus(q, df, 0, *slots)
            partial[where, rows_of(q), :] = total.astype(jnp.bfloat16)
            if turn == 0:
                rs_copy(q, block(partial, q, df, 0), 12, True, d).start()
            elif turn == 1:
                rs_copy(q, block(partial, q, df, 0), 13, True, -d).start()
            elif turn == 2:
                rs_copy(q, block(partial, q, df, 0), 14, True, d).start()

    for q in quarters:
        rs_wait(q, 13)
        rs_wait(q, 14)
        _, total = plus(q, 0, 0, 13, 14)
        result[rows_of(q), :] = total.astype(jnp.bfloat16)
        if q == 3:
            shared_sum[...] = total[160:288, :]

        def send_back(other, carry):
            @pl.when(other != e)
            def _():
                pltpu.make_async_remote_copy(
                    result.at[pl.ds(pl.multiple_of(other * 32, 32), 32)],
                    returned.at[at_e],
                    back_send,
                    back_recv,
                    device_id={"ep": other},
                    device_id_type=MESH,
                ).start()

            return carry

        lax.fori_loop(q * 9, min(ep_count, (q + 1) * 9), send_back, 0)
    returned[at_e, :] = result[at_e, :]
    pltpu.make_async_copy(
        returned.at[pl.ds(0, 992)], returned.at[pl.ds(0, 992)], back_recv
    ).wait()
    combined = (
        shared_sum[...]
        + jnp.dot(comb[0], returned[...], preferred_element_type=jnp.float32)
        + jnp.dot(comb[1], returned[...], preferred_element_type=jnp.float32)
    )
    for k in range(tp_count):
        cut_back[k] = combined[k * rows : (k + 1) * rows, :].astype(jnp.bfloat16)

    def send_fin(k, carry):
        other, device = tp_peer(k)
        pltpu.make_async_remote_copy(
            cut_back.at[other],
            landed.at[t],
            fin_send,
            fin_recv,
            device_id=device,
            device_id_type=MESH,
        ).start()
        return carry

    lax.fori_loop(1, tp_count, send_fin, 0)
    landed[t] = cut_back[t]

    most = tp_count - 1
    for ref, sem in (
        (pre.at[pl.ds(0, most)], pre_send),
        (mixes.at[pl.ds(0, most)], mix_send),
        (outgoing.at[pl.ds(0, 992)], go_send),
        (pooled.at[pl.ds(0, most)], ag_send),
        (partial.at[pl.ds(0, most)], rs_send),
        (result.at[pl.ds(0, 992)], back_send),
        (landed.at[pl.ds(0, most)], fin_recv),
        (landed.at[pl.ds(0, most)], fin_send),
    ):
        pltpu.make_async_copy(ref, ref, sem).wait()
    for k in range(tp_count):
        out[:, k * 128 : (k + 1) * 128] = landed[k]


def expert_half(
    moe_in,
    norm_gain,
    route_ids,
    route_weights,
    gate_weight,
    up_weight,
    down_weight,
    shared_gate,
    shared_up,
    shared_down,
):
    own_rows, width = moe_in.shape
    hidden = gate_weight.shape[1]
    bf16, f32 = jnp.bfloat16, jnp.float32
    vmem, dma = pltpu.VMEM, pltpu.SemaphoreType.DMA
    here, there = pl.BlockSpec(memory_space=pltpu.VMEM), pl.BlockSpec(memory_space=pl.ANY)
    return pl.pallas_call(
        expert_kernel,
        out_shape=jax.ShapeDtypeStruct((own_rows, width), bf16),
        in_specs=[here] * 5 + [there] * 6,
        out_specs=here,
        scratch_shapes=[
            vmem((4, hidden, width), bf16),
            vmem((2, hidden, width), bf16),
            vmem((3, hidden, width), bf16),
            vmem((16, own_rows, 128), bf16),
            vmem((16, own_rows, 128), f32),
            vmem((16, own_rows, 128), bf16),
            vmem((1024, 128), bf16),
            vmem((16, 1152, 128), bf16),
            vmem((16, 1152, 128), bf16),
            vmem((4, 15, 288, 128), bf16),
            vmem((1152, 128), bf16),
            vmem((128, 128), f32),
            vmem((1024, 128), bf16),
            vmem((2, 128, 1024), bf16),
            vmem((16, own_rows, 128), bf16),
            vmem((16, own_rows, 128), bf16),
            dma((6,)),
            dma,
            dma,
            dma,
            dma,
            dma,
            dma,
            dma,
            dma((4, 16)),
            dma,
            dma((4, 15)),
            dma,
            dma,
            dma,
            dma,
        ],
        compiler_params=pltpu.CompilerParams(
            collective_id=0, has_side_effects=True, vmem_limit_bytes=40 * 1024 * 1024
        ),
        cost_estimate=pl.CostEstimate(
            flops=80_000_000_000, bytes_accessed=200_000_000, transcendentals=300_000
        ),
    )(
        moe_in,
        norm_gain[None, :],
        route_ids,
        route_ids.T,
        route_weights,
        gate_weight,
        up_weight,
        down_weight,
        shared_gate,
        shared_up,
        shared_down,
    )


def shards(
    queries,
    keys,
    values,
    key_bias,
    moe_in,
    norm_gain,
    route_ids,
    route_weights,
    gate_weight,
    up_weight,
    down_weight,
    shared_gate,
    shared_up,
    shared_down,
):
    heads_out = stick_half(queries, keys, values, key_bias)
    moe_out = expert_half(
        moe_in,
        norm_gain,
        route_ids,
        route_weights,
        gate_weight,
        up_weight,
        down_weight,
        shared_gate,
        shared_up,
        shared_down,
    )
    return (heads_out, moe_out)


def solution(mesh):
    split = Mesh(mesh.devices.reshape(mesh.shape["ep"], 4, 4), ("ep", "tp_0", "tp_1"))
    return jax.shard_map(
        shards,
        mesh=split,
        in_specs=(
            P("ep", TP),
            P("ep", TP),
            P("ep", TP),
            P("ep", TP),
            P(EP_TP, None),
            P(),
            P("ep", None),
            P(EP_TP, None),
            P("ep", TP, None),
            P("ep", TP, None),
            P("ep", TP, None),
            P(TP, None),
            P(TP, None),
            P(TP, None),
        ),
        out_specs=(P("ep", TP), P(EP_TP, None)),
        check_vma=False,
    )
```

time: 327 us -> 184 us (0.56)
  waiting for transfers between devices: 127 us -> 0.04 us
  Pallas kernels: 42.5 us -> 154 us
  blocking collectives: 87.4 us -> 0 us
  starting transfers between devices: 13.6 us -> 0.04 us
  matrix products: 11 us -> 0 us
  other arithmetic: 10.6 us -> 2.34 us
  local copies, waits for them, and re-layouts: 18.6 us -> 13.1 us
    pallas_call x0 -> x1, Pallas kernels: none -> 111 us  [expert_half(): pl.pallas_call(expert_kernel, out_shape=jax.ShapeDtypeStruct((own_rows, w...]
    reduce_scatter x2 -> x0, waiting for transfers between devices: 88.6 us -> none  [summed_rows(): so_far = lax.psum_scatter(so_far, axis, scatter_dimension=0, tiled=True)]
    all_to_all x2 -> x0, blocking collectives: 87.4 us -> none  [the longest x1 62.5 us: from_everyone(): return lax.all_to_all(copies, axis, split_axis=0, concat_axis=0, tiled=True)]
    all_gather x1, waiting for transfers between devices: 37.9 us -> 0.02 us  [stick_half(): lax.all_gather(packed_rows(keys, values, key_bias), 'ep', axis=0, tiled=F...]
    all_to_all x1 -> x0, starting transfers between devices: 13.5 us -> none  [expert_half(): lax.all_to_all(slot_out, 'ep', split_axis=1, concat_axis=1, tiled=True)]
    dot_general x4 -> x0, matrix products: 11 us -> none  [the longest x1 6.53 us: expert_terms(): jnp.einsum('besf,efd->besd', hidden, down_weight, preferred_element_type=...]
    unnamed x30 -> x25, local copies, waits for them, and re-layouts: 7.91 us -> 13.1 us
    concatenate x2 -> x0, other arithmetic: 5.05 us -> none  [the longest x1 5.02 us: expert_terms(): return jnp.concatenate([routed_out, shared_out], axis=1).reshape(-1, width)]
  transfers between devices with their start and end apart: 4 -> 1, of which waited for: 3 -> 0; matrix products, arithmetic and copies ran while one was open for 1% -> 1% of each run, Pallas kernels for 13% -> 61%
where the time goes in v2:
time: 184 us; the launch traced here: 183 us
  Pallas kernels  154 us (84%)
  between operations  14.1 us (8%)
  local copies, waits for them, and re-layouts  13.1 us (7%)
  other arithmetic  2.34 us (1%)
    pallas_call x1, Pallas kernels, expert_half(): pl.pallas_call(expert_kernel, out_shape=jax.ShapeDtypeStruct((own_rows, w...  111 us
    pallas_call x1, Pallas kernels, stick_half(): pl.pallas_call(functools.partial(attention_kernel, width ** (-0.5)), out_...  42.5 us
    unnamed x25, local copies, waits for them, and re-layouts  13.1 us
  transfers between devices with their start and end apart: 1, of which 0 were waited for; matrix products, arithmetic and copies ran while one was open for 1% of the time, Pallas kernels for 61%

profile of v2, /device:TPU:481, one launch (start us, length us, event | category | flops | bytes accessed | tf_op | source)
XLA Modules:
  0.0 183.2 jit_solution(12407149924323519787)
XLA Ops:
  7.2 0.0 all-gather.3.cloned.1.call-start
  7.2 0.7 reduce
  7.9 1.6 fusion.1
  9.6 0.0 all-gather.3.cloned.1.call-update
  9.6 0.8 copy.16.ids
  10.4 0.8 copy.17.mix
  11.1 0.0 copy-start
  11.1 0.7 copy-done
  11.8 0.0 copy-start.2
  11.8 1.0 copy-done.2
  12.8 0.0 copy-start.3
  12.9 1.0 copy-done.3
  13.9 0.0 copy-start.4
  13.9 1.0 copy-done.4
  14.9 0.0 copy-start.5
  14.9 0.9 copy-done.5
  15.9 0.0 copy-start.6
  15.9 0.9 copy-done.6
  16.8 0.0 copy-start.7
  16.8 0.9 copy-done.7
  17.8 0.0 copy-start.9
  17.8 0.8 copy-done.9
  18.5 0.0 copy-start.10
  18.5 0.7 copy-done.10
  19.2 0.0 copy-start.8
  19.2 111.1 %shard_map.150 = bf16[8,2048]{1,0:T(8,128)(2,1)S(1)} custom-call(bf16[8,2048]{1,0:T(8,128)(2,1)S(1)} %copy-done.9, f32[1,2048]{1,0:T(1,128)S(1)} %bitcast.6, s32[128,4]{1,0:T(8,128)S(1)} %copy.16.ids, s32[4,128]{1,0:T(4,128)S(1)} %bitcast.4, f32[8,4]{1,0:T(8,128)S(1)} %copy.17.mix, bf16[2,64,2048]{2,1,0:T(8,128)(2,1)S(1)} %copy-done.2, ...), custom_call_target="tpu_custom_call" | custom-call | flops 80000000000 | bytes 200000000 | tf_op jit(solution)/shard_map/pallas_call | solution.py:538
  130.4 0.0 all-gather.3.cloned.1.call-done
  130.4 0.0 copy-done.8
  130.4 0.0 copy-start.1
  130.4 2.8 %copy-done.1 = bf16[25088,128]{1,0:T(8,128)(2,1)S(1)} copy-done((bf16[25088,128]{1,0:T(8,128)(2,1)S(1)}, bf16[25088,128]{1,0:T(8,128)(2,1)}, u32[]{:S(2)}) %copy-start.1) | copy-done | bytes 6422552
  133.2 42.5 %shard_map.149 = bf16[384,128]{1,0:T(8,128)(2,1)} custom-call(bf16[384,128]{1,0:T(8,128)(2,1)S(1)} %copy-done.8, bf16[32,784,128]{2,1,0:T(8,128)(2,1)S(1)} %bitcast.5), custom_call_target="tpu_custom_call" | custom-call | flops 8000000000 | bytes 7000000 | tf_op jit(solution)/shard_map/pallas_call | solution.py:92
  175.7 0.6 copy.19
Async XLA Ops:
  7.2 123.2 %all-gather.3.cloned.1.call-start = ((), (), s32[]{:S(2)}) async-start(), calls=%async_computation | async-start | bytes 6623232 | tf_op jit(solution)/shard_map/all_gather | solution.py:91
  11.1 0.7 copy-start
  11.8 1.0 copy-start.2
  12.8 1.0 copy-start.3
  13.9 1.0 copy-start.4
  14.9 0.9 copy-start.5
  15.9 0.9 copy-start.6
  16.8 0.9 copy-start.7
  17.8 0.8 copy-start.9
  18.5 0.7 copy-start.10
  19.2 111.1 %copy-start.8 = (bf16[384,128]{1,0:T(8,128)(2,1)S(1)}, bf16[384,128]{1,0:T(8,128)(2,1)}, u32[]{:S(2)}) copy-start(bf16[384,128]{1,0:T(8,128)(2,1)} %q_ref.1) | copy-start | bytes 294916
  130.4 2.8 %copy-start.1 = (bf16[25088,128]{1,0:T(8,128)(2,1)S(1)}, bf16[25088,128]{1,0:T(8,128)(2,1)}, u32[]{:S(2)}) copy-start(bf16[25088,128]{1,0:T(8,128)(2,1)} %all-gather.3.cloned.1.call-done) | copy-start | bytes 19267588
Sparse Core Ops, SparseCore 0:
  10.1 83.2 all-gather.2

commit v3 on v2

--- a/solution.py
+++ b/solution.py
@@ -24,82 +24,135 @@
     )
 
 
-def attention_kernel(scale_factor, q_ref, kv_ref, o_ref, tri, acc, later):
-    num_rows, width = q_ref.shape
-    chunk = 128
-    me = lax.axis_index("ep")
-    row_id = lax.broadcasted_iota(jnp.int32, (num_rows, num_rows + 128), 0)
-    col_id = lax.broadcasted_iota(jnp.int32, (num_rows, num_rows + 128), 1)
-    tri[...] = jnp.where((row_id > col_id) | (col_id >= num_rows), -1.0, 0.0).astype(jnp.bfloat16)
+FAR = -1e30
+
+
+def attention_start(state, row_count):
+    scores_ref, logit_ref, sums_ref, soft_ref, weight_ref, tri, acc, later = state
+    row_id = lax.broadcasted_iota(jnp.int32, tri.shape, 0)
+    col_id = lax.broadcasted_iota(jnp.int32, tri.shape, 1)
+    tri[...] = jnp.where((row_id > col_id) | (col_id >= 128), -1.0, 0.0).astype(jnp.bfloat16)
     acc[...] = jnp.zeros_like(acc)
     later[...] = jnp.zeros_like(later)
-
-    def visit(block, diagonal):
-        k_block = kv_ref[block, :num_rows, :]
-        v_block = kv_ref[block, num_rows : 2 * num_rows, :]
-        bias = kv_ref[block, 2 * num_rows : 2 * num_rows + 16, :].astype(jnp.float32)
-        bias = jnp.concatenate([bias[r : r + 1] for r in range(num_rows // width)], axis=1)
-        for first in range(0, num_rows, chunk):
-            rows = slice(first, first + chunk)
-            scores = (
-                lax.dot_general(
-                    q_ref[rows, :],
-                    k_block,
-                    (((1,), (1,)), ((), ())),
-                    preferred_element_type=jnp.float32,
-                )
-                * scale_factor
-                + bias
+    sums_ref[...] = jnp.zeros_like(sums_ref)
+    logit_ref[...] = jnp.full(logit_ref.shape, FAR, jnp.float32)
+    scores_ref[...] = jnp.full(scores_ref.shape, FAR, jnp.float32)
+
+
+def attention_finish_block(state, v_block):
+    scores_ref, logit_ref, sums_ref, soft_ref, weight_ref, tri, acc, later = state
+    num_rows = scores_ref.shape[0]
+    piece = 16
+    for first in range(0, num_rows, piece):
+        carried = later[first : first + piece, :]
+        for c in reversed(range(num_rows // 128)):
+            at = c * num_rows + first
+            weight_ref[first : first + piece, c * 128 : (c + 1) * 128] = jnp.exp(
+                logit_ref[first : first + piece, c * 128 : (c + 1) * 128]
+                + (sums_ref[at : at + piece, :128] + carried)
+            ).astype(jnp.bfloat16)
+            carried = carried + sums_ref[at : at + piece, 128:]
+        later[first : first + piece, :] = carried
+    acc[...] += jnp.dot(weight_ref[...], v_block, preferred_element_type=jnp.float32)
+
+
+def attention_sum_block(state):
+    scores_ref, logit_ref, sums_ref, soft_ref, weight_ref, tri, acc, later = state
+    num_rows = scores_ref.shape[0]
+    piece = 16
+    for c in range(num_rows // 128):
+        columns = slice(c * 128, (c + 1) * 128)
+        for first in range(0, num_rows, piece):
+            scores = scores_ref[first : first + piece, columns]
+            soft = jnp.maximum(scores, jnp.log(1.0 + jnp.exp(jnp.minimum(scores, 88.0))))
+            logit_ref[first : first + piece, columns] = scores - soft
+            soft_ref[c * num_rows + first : c * num_rows + first + piece, :] = soft.astype(
+                jnp.bfloat16
             )
-            soft = jnp.maximum(scores, jnp.log(1.0 + jnp.exp(jnp.minimum(scores, 88.0))))
-            dropped = soft
-            if diagonal:
-                causal = lax.broadcasted_iota(
-                    jnp.int32, scores.shape, 1
-                ) < first + lax.broadcasted_iota(jnp.int32, scores.shape, 0)
-                dropped = jnp.where(causal, soft, 0.0)
-            sums = jnp.dot(
-                dropped.astype(jnp.bfloat16), tri[...], preferred_element_type=jnp.float32
-            )
-            carried = later[rows, :]
-            between = sums[:, :num_rows] + jnp.concatenate(
-                [carried] * (num_rows // width), axis=1
-            )
-            weights = jnp.exp(scores - soft + between)
-            if diagonal:
-                weights = jnp.where(causal, weights, 0.0)
-            acc[rows, :] += jnp.dot(
-                weights.astype(jnp.bfloat16), v_block, preferred_element_type=jnp.float32
-            )
-            later[rows, :] = carried + sums[:, num_rows:]
-
-    visit(me, True)
-
-    def earlier(count, carry):
-        visit(me - 1 - count, False)
-        return carry
-
-    lax.fori_loop(0, me, earlier, 0)
-    raw_out = acc[...]
+    sums_ref[...] = jnp.dot(soft_ref[...], tri[...], preferred_element_type=jnp.float32)
+
+
+def attention_score_block(state, q_ref, k_block, bias_rows, diagonal):
+    scores_ref = state[0]
+    num_rows, width = q_ref.shape
+    bias = bias_rows.astype(jnp.float32)
+    bias = jnp.concatenate([bias[r : r + 1] for r in range(num_rows // width)], axis=1)
+    products = lax.dot_general(
+        q_ref[...], k_block, (((1,), (1,)), ((), ())), preferred_element_type=jnp.float32
+    )
+    scores = products * width ** (-0.5) + bias
+    if diagonal:
+        causal = lax.broadcasted_iota(jnp.int32, scores.shape, 1) < lax.broadcasted_iota(
+            jnp.int32, scores.shape, 0
+        )
+        scores = jnp.where(causal, scores, FAR)
+    scores_ref[...] = scores
+
+
+def attention_parts(kv_ref, block, num_rows):
+    return (
+        kv_ref[block, :num_rows, :],
+        kv_ref[block, num_rows : 2 * num_rows, :],
+        kv_ref[block, 2 * num_rows : 2 * num_rows + 16, :],
+    )
+
+
+def attention_step(state, q_ref, kv_ref, me, count):
+    num_rows = q_ref.shape[0]
+    v_block = attention_parts(kv_ref, jnp.minimum(me - count + 2, me), num_rows)[1]
+    k_block, _, bias_rows = attention_parts(kv_ref, jnp.maximum(me - count, 0), num_rows)
+    attention_finish_block(state, v_block)
+    attention_sum_block(state)
+    attention_score_block(state, q_ref, k_block, bias_rows, False)
+
+
+def attention_end(state, o_ref):
+    raw_out = state[6][...]
     o_ref[...] = (
         raw_out * lax.rsqrt(jnp.mean(raw_out * raw_out, axis=1, keepdims=True) + norm_eps)
     ).astype(jnp.bfloat16)
+
+
+def attention_kernel(q_ref, kv_ref, o_ref, *state):
+    num_rows = q_ref.shape[0]
+    me = lax.axis_index("ep")
+    attention_start(state, num_rows)
+    k_block, _, bias_rows = attention_parts(kv_ref, me, num_rows)
+    attention_score_block(state, q_ref, k_block, bias_rows, True)
+
+    def step(count, carry):
+        attention_step(state, q_ref, kv_ref, me, count)
+        return carry
+
+    lax.fori_loop(1, me + 3, step, 0)
+    attention_end(state, o_ref)
+
+
+def attention_state(num_rows, width):
+    f32, bf16 = jnp.float32, jnp.bfloat16
+    pieces = num_rows // 128
+    return [
+        pltpu.VMEM((num_rows, num_rows), f32),
+        pltpu.VMEM((num_rows, num_rows), f32),
+        pltpu.VMEM((pieces * num_rows, 256), f32),
+        pltpu.VMEM((pieces * num_rows, 128), bf16),
+        pltpu.VMEM((num_rows, num_rows), bf16),
+        pltpu.VMEM((128, 256), bf16),
+        pltpu.VMEM((num_rows, width), f32),
+        pltpu.VMEM((num_rows, 128), f32),
+    ]
 
 
 def stick_half(queries, keys, values, key_bias):
     num_rows, width = queries.shape
     filled = lax.all_gather(packed_rows(keys, values, key_bias), "ep", axis=0, tiled=False)
     return pl.pallas_call(
-        functools.partial(attention_kernel, width ** (-0.5)),
+        attention_kernel,
         out_shape=jax.ShapeDtypeStruct((num_rows, width), jnp.bfloat16),
         in_specs=[pl.BlockSpec(memory_space=pltpu.VMEM)] * 2,
         out_specs=pl.BlockSpec(memory_space=pltpu.VMEM),
-        scratch_shapes=[
-            pltpu.VMEM((num_rows, num_rows + 128), jnp.bfloat16),
-            pltpu.VMEM((num_rows, width), jnp.float32),
-            pltpu.VMEM((num_rows, 128), jnp.float32),
-        ],
-        compiler_params=pltpu.CompilerParams(vmem_limit_bytes=40 * 1024 * 1024),
+        scratch_shapes=attention_state(num_rows, width),
+        compiler_params=pltpu.CompilerParams(vmem_limit_bytes=60 * 1024 * 1024),
         cost_estimate=pl.CostEstimate(
             flops=8_000_000_000, bytes_accessed=7_000_000, transcendentals=14_000_000
         ),
@@ -574,7 +627,7 @@
             dma,
         ],
         compiler_params=pltpu.CompilerParams(
-            collective_id=0, has_side_effects=True, vmem_limit_bytes=40 * 1024 * 1024
+            collective_id=0, has_side_effects=True, vmem_limit_bytes=60 * 1024 * 1024
         ),
         cost_estimate=pl.CostEstimate(
             flops=80_000_000_000, bytes_accessed=200_000_000, transcendentals=300_000

time: 184 us -> 155 us (0.84)
  Pallas kernels: 154 us -> 135 us
  local copies, waits for them, and re-layouts: 13.1 us -> 3.38 us
    pallas_call x1, Pallas kernels: 42.5 us -> 24 us  [stick_half(): pl.pallas_call(attention_kernel, out_shape=jax.ShapeDtypeStruct((num_rows...]
    unnamed x25 -> x5, local copies, waits for them, and re-layouts: 13.1 us -> 3.38 us
  transfers between devices with their start and end apart: 1 -> 1, of which waited for: 0 -> 0; matrix products, arithmetic and copies ran while one was open for 1% -> 2% of each run, Pallas kernels for 61% -> 72%
where the time goes in v3:
time: 155 us
  Pallas kernels  135 us (87%)
  between operations  14.1 us (9%)
  local copies, waits for them, and re-layouts  3.38 us (2%)
  other arithmetic  2.32 us (1%)
    pallas_call x1, Pallas kernels, expert_half(): pl.pallas_call(expert_kernel, out_shape=jax.ShapeDtypeStruct((own_rows, w...  111 us
    pallas_call x1, Pallas kernels, stick_half(): pl.pallas_call(attention_kernel, out_shape=jax.ShapeDtypeStruct((num_rows...  24 us
    unnamed x5, local copies, waits for them, and re-layouts  3.38 us
  transfers between devices with their start and end apart: 1, of which 0 were waited for; matrix products, arithmetic and copies ran while one was open for 2% of the time, Pallas kernels for 72%

profile of v3, /device:TPU:481, one launch (start us, length us, event | category | flops | bytes accessed | tf_op | source)
XLA Modules:
  0.0 154.7 jit_solution(11645943904442132088)
XLA Ops:
  7.2 0.0 all-gather.3.cloned.1.call-start
  7.2 0.7 reduce
  7.9 1.6 %fusion.1 = bf16[784,128]{1,0:T(8,128)(2,1)} fusion(bf16[3,128]{1,0:T(4,128)(2,1)S(1)} %bitcast.4, bf16[384,128]{1,0:T(8,128)(2,1)} %param.16, bf16[384,128]{1,0:T(8,128)(2,1)} %param.15), kind=kLoop, calls=%fused_computation.2 | loop fusion | flops 802816 | bytes 398080 | tf_op jit(solution)/shard_map/concatenate | solution.py:22
  9.5 0.0 all-gather.3.cloned.1.call-update
  9.6 1.4 copy.16.ids
  11.0 1.3 copy.17.mix
  12.3 110.9 %shard_map.150 = bf16[8,2048]{1,0:T(8,128)(2,1)} custom-call(bf16[8,2048]{1,0:T(8,128)(2,1)} %moe_in.1, f32[1,2048]{1,0:T(1,128)} %bitcast.7, s32[128,4]{1,0:T(8,128)} %copy.16.ids, s32[4,128]{1,0:T(4,128)} %bitcast.5, f32[8,4]{1,0:T(8,128)} %copy.17.mix, bf16[2,64,2048]{2,1,0:T(8,128)(2,1)} %gate.1, bf16[2,64,2048]{2,1,0:T(8,128)(2,1)} %up.1, ...), custom_call_target="tpu_custom_call" | custom-call | flops 80000000000 | bytes 200000000 | tf_op jit(solution)/shard_map/pallas_call | solution.py:591
  123.2 0.0 all-gather.3.cloned.1.call-done
  123.2 0.0 copy-start
  123.2 24.0 %shard_map.149 = bf16[384,128]{1,0:T(8,128)(2,1)} custom-call(bf16[384,128]{1,0:T(8,128)(2,1)} %q_ref.1, bf16[32,784,128]{2,1,0:T(8,128)(2,1)} %bitcast.6), custom_call_target="tpu_custom_call" | custom-call | flops 8000000000 | bytes 7000000 | tf_op jit(solution)/shard_map/pallas_call | solution.py:149
  147.2 0.0 copy-done
  147.2 0.6 copy.19
Async XLA Ops:
  7.2 116.1 %all-gather.3.cloned.1.call-start = ((), (), s32[]{:S(2)}) async-start(), calls=%async_computation | async-start | bytes 6623232 | tf_op jit(solution)/shard_map/all_gather | solution.py:148
  123.2 24.0 %copy-start = (bf16[8,2048]{1,0:T(8,128)(2,1)S(1)}, bf16[8,2048]{1,0:T(8,128)(2,1)}, u32[]{:S(2)}) copy-start(bf16[8,2048]{1,0:T(8,128)(2,1)} %shard_map.150) | copy-start | bytes 98308
Sparse Core Ops, SparseCore 0:
  10.1 81.9 all-gather.2

commit v4 on v3

--- a/solution.py
+++ b/solution.py
@@ -14,14 +14,6 @@
 
 norm_eps = 1e-05
 MESH = pl.DeviceIdType.MESH
-
-
-def packed_rows(keys, values, key_bias):
-    num_rows, width = keys.shape
-    bias_rows = key_bias.reshape(num_rows // width, width)
-    return jnp.concatenate(
-        [keys, values, jnp.pad(bias_rows, ((0, 16 - bias_rows.shape[0]), (0, 0)))], axis=0
-    )
 
 
 FAR = -1e30
@@ -113,21 +105,6 @@
     ).astype(jnp.bfloat16)
 
 
-def attention_kernel(q_ref, kv_ref, o_ref, *state):
-    num_rows = q_ref.shape[0]
-    me = lax.axis_index("ep")
-    attention_start(state, num_rows)
-    k_block, _, bias_rows = attention_parts(kv_ref, me, num_rows)
-    attention_score_block(state, q_ref, k_block, bias_rows, True)
-
-    def step(count, carry):
-        attention_step(state, q_ref, kv_ref, me, count)
-        return carry
-
-    lax.fori_loop(1, me + 3, step, 0)
-    attention_end(state, o_ref)
-
-
 def attention_state(num_rows, width):
     f32, bf16 = jnp.float32, jnp.bfloat16
     pieces = num_rows // 128
@@ -143,35 +120,25 @@
     ]
 
 
-def stick_half(queries, keys, values, key_bias):
-    num_rows, width = queries.shape
-    filled = lax.all_gather(packed_rows(keys, values, key_bias), "ep", axis=0, tiled=False)
-    return pl.pallas_call(
-        attention_kernel,
-        out_shape=jax.ShapeDtypeStruct((num_rows, width), jnp.bfloat16),
-        in_specs=[pl.BlockSpec(memory_space=pltpu.VMEM)] * 2,
-        out_specs=pl.BlockSpec(memory_space=pltpu.VMEM),
-        scratch_shapes=attention_state(num_rows, width),
-        compiler_params=pltpu.CompilerParams(vmem_limit_bytes=60 * 1024 * 1024),
-        cost_estimate=pl.CostEstimate(
-            flops=8_000_000_000, bytes_accessed=7_000_000, transcendentals=14_000_000
-        ),
-    )(queries, filled)
-
-
-def expert_kernel(
+def both_kernel(
+    queries,
+    keys,
+    values,
+    bias_rows,
     moe_in,
     gain,
-    ids,
     ids_across,
-    mix,
+    mix_across,
     gate,
     up,
     down,
     shared_gate,
     shared_up,
     shared_down,
+    heads,
     out,
+    kv,
+    turned,
     w_in,
     w_out,
     w_shared,
@@ -203,6 +170,13 @@
     back_recv,
     fin_send,
     fin_recv,
+    up_send,
+    up_recv,
+    down_send,
+    down_recv,
+    pair_send,
+    pair_recv,
+    *state,
 ):
     ep_count, tp_count = lax.axis_size("ep"), 16
     rows = moe_in.shape[0]
@@ -249,14 +223,25 @@
     ).astype(jnp.bfloat16)
     for k in range(tp_count):
         cut[k] = normed[:, k * 128 : (k + 1) * 128]
-    own_ids = ids[pl.ds(pl.multiple_of(t * rows, rows), rows), :]
-    own_mix = mix[...]
-    lane = lax.broadcasted_iota(jnp.int32, (rows, 128), 1)
+    top_k = ids_across.shape[0]
+    turned[...] = jnp.zeros_like(turned)
+    turned[0, :top_k, :] = ids_across[...].astype(jnp.float32)
+    turned[1, :top_k, :rows] = mix_across[...]
+    own_mix = turned[1].T[:rows, :]
+    turned[0] = turned[0].T
+    own_ids = turned[0, pl.ds(pl.multiple_of(t * rows, rows), rows), :]
+    lane = lax.broadcasted_iota(jnp.int32, (rows, 128), 1).astype(jnp.float32)
     spread = jnp.zeros((rows, 128), jnp.float32)
-    for k in range(mix.shape[1]):
+    for k in range(top_k):
         spread = spread + jnp.where(own_ids[:, k : k + 1] == lane, own_mix[:, k : k + 1], 0.0)
     mixes[t] = spread
     pre[t] = cut[t]
+
+    tokens = queries.shape[0]
+    kv[e, :tokens, :] = keys[...]
+    kv[e, tokens : 2 * tokens, :] = values[...]
+    kv[e, 2 * tokens : 2 * tokens + 16, :] = bias_rows[...]
+    attention_start(state, tokens)
 
     pl.semaphore_wait(barrier, ep_count + tp_count - 2)
 
@@ -316,6 +301,92 @@
 
     lax.fori_loop(1, ep_count, send_go, 0)
     pooled[t, at_e, :] = outgoing[at_e, :]
+
+    chips = ep_count // 2
+    z, core = e // 2, lax.rem(e, 2)
+    partner = e + 1 - 2 * core
+    most_up, most_down = chips // 2, chips // 2 - 1
+
+    def kv_copy(chip, target, send_sem, recv_sem):
+        ref = kv.at[chip * 2 + core]
+        return pltpu.make_async_remote_copy(
+            ref, ref, send_sem, recv_sem, device_id={"ep": target}, device_id_type=MESH
+        )
+
+    def chip_at(step):
+        return lax.rem(z + step + chips, chips)
+
+    def up_copy(n):
+        return kv_copy(
+            chip_at(-n), chip_at(1) * 2 + core, up_send.at[n], up_recv.at[n + 1]
+        )
+
+    def down_copy(n):
+        return kv_copy(
+            chip_at(n), chip_at(-1) * 2 + core, down_send.at[n], down_recv.at[n + 1]
+        )
+
+    def pair_copy(chip):
+        return kv_copy(chip, partner, pair_send.at[chip], pair_recv.at[chip])
+
+    def goes_up(n):
+        return (z - n >= 0) & (z < chips - 1)
+
+    def goes_down(n):
+        return chip_at(n) < most_down
+
+    @pl.when(core == 0)
+    def _():
+        pair_copy(z).start()
+
+    @pl.when(goes_up(0))
+    def _():
+        up_copy(0).start()
+
+    @pl.when(goes_down(0))
+    def _():
+        down_copy(0).start()
+
+    def kv_service(n):
+        @pl.when(z >= n)
+        def _():
+            up_copy(n - 1).wait_recv()
+            pair_copy(z - n).start()
+
+        if n < most_up:
+
+            @pl.when(goes_up(n))
+            def _():
+                up_copy(n).start()
+
+        if n <= most_down:
+
+            @pl.when(goes_down(n))
+            def _():
+                down_copy(n - 1).wait_recv()
+
+                @pl.when(chip_at(n) < z)
+                def _():
+                    pair_copy(chip_at(n)).start()
+
+                if n < most_down:
+                    down_copy(n).start()
+
+    def attend(first, last):
+        def pair(n, carry):
+            @pl.when(z >= n)
+            def _():
+                pair_wait(z - n)
+                for extra in range(2):
+                    attention_step(state, queries, kv, e, 2 * n - 1 + core + extra)
+
+            return carry
+
+        lax.fori_loop(first, last + 1, pair, 0)
+
+    def pair_wait(chip):
+        ref = kv.at[chip * 2 + 1 - core]
+        pltpu.make_async_copy(ref, ref, pair_recv.at[chip]).wait()
 
     pltpu.make_async_copy(
         mixes.at[pl.ds(0, tp_count - 1)], mixes.at[pl.ds(0, tp_count - 1)], mix_recv
@@ -333,6 +404,9 @@
             comb[part, :, k * 256 : (k + 1) * 256] = jnp.where(keep, wide, 0.0).astype(
                 jnp.bfloat16
             )
+
+    k_block, _, own_bias = attention_parts(kv, e, tokens)
+    attention_score_block(state, queries, k_block, own_bias, True)
 
     pltpu.make_async_copy(
         pooled.at[t, pl.ds(0, 992)], pooled.at[t, pl.ds(0, 992)], go_recv
@@ -401,12 +475,21 @@
         ag_wait(q, 2, 0)
         ag_copy(q, 2, 0, False, 1).start()
         ag_copy(q, 2, 0, False, 3).start()
+    kv_service(1)
+
+    @pl.when(core == 1)
+    def _():
+        pair_wait(z)
+        attention_step(state, queries, kv, e, 1)
+
     for hop in range(3):
         for q in quarters:
             d = axes(q)[2]
             df = (-d, d, 2)[hop]
             ag_wait(q, df, -d)
             ag_copy(q, df, -d, False, d).start()
+        if hop > 0:
+            kv_service(hop + 1)
 
     for load in loads:
         load.wait()
@@ -477,6 +560,10 @@
             rs_copy(q, block(partial, q, df, 2), slot, False, d).start()
             rs_copy(q, block(partial, q, df, -d), slot + 1, False, -d).start()
 
+    kv_service(4)
+    attend(1, 3)
+    kv_service(5)
+    attend(4, 4)
     rows_of = lambda q: slice(q * quarter, (q + 1) * quarter)
     for turn in range(4):
         for q in quarters:
@@ -486,6 +573,9 @@
             where, total = plus(q, df, d, df * 3)
             partial[where, rows_of(q), :] = total.astype(jnp.bfloat16)
             rs_copy(q, block(partial, q, df, d), df * 3 + 2, False, d).start()
+        if turn < 3:
+            kv_service(turn + 6)
+        attend(turn + 5, turn + 5)
     for turn in range(4):
         for q in quarters:
             d = axes(q)[2]
@@ -504,6 +594,8 @@
                 rs_copy(q, block(partial, q, df, 0), 13, True, -d).start()
             elif turn == 2:
                 rs_copy(q, block(partial, q, df, 0), 14, True, d).start()
+        if turn < 3:
+            attend(turn + 9, turn + 9)
 
     for q in quarters:
         rs_wait(q, 13)
@@ -529,6 +621,10 @@
 
         lax.fori_loop(q * 9, min(ep_count, (q + 1) * 9), send_back, 0)
     returned[at_e, :] = result[at_e, :]
+    attend(12, chips - 1)
+    for extra in range(2):
+        attention_step(state, queries, kv, e, e + 1 + extra)
+    attention_end(state, heads)
     pltpu.make_async_copy(
         returned.at[pl.ds(0, 992)], returned.at[pl.ds(0, 992)], back_recv
     ).wait()
@@ -567,11 +663,38 @@
         (landed.at[pl.ds(0, most)], fin_send),
     ):
         pltpu.make_async_copy(ref, ref, sem).wait()
+
+    @pl.when(core == 0)
+    def _():
+        pair_copy(z).wait_send()
+
+    for n in range(most_up):
+
+        @pl.when(goes_up(n))
+        def _():
+            up_copy(n).wait_send()
+
+    for n in range(most_down):
+
+        @pl.when(goes_down(n))
+        def _():
+            down_copy(n).wait_send()
+
+    for n in range(1, chips):
+
+        @pl.when(z >= n)
+        def _():
+            pair_copy(z - n).wait_send()
+
     for k in range(tp_count):
         out[:, k * 128 : (k + 1) * 128] = landed[k]
 
 
-def expert_half(
+def both_halves(
+    queries,
+    keys,
+    values,
+    key_bias,
     moe_in,
     norm_gain,
     route_ids,
@@ -584,16 +707,24 @@
     shared_down,
 ):
     own_rows, width = moe_in.shape
+    tokens, head_dim = queries.shape
+    bias_rows = key_bias.reshape(tokens // head_dim, head_dim)
+    bias_rows = jnp.pad(bias_rows, ((0, 16 - tokens // head_dim), (0, 0)))
     hidden = gate_weight.shape[1]
     bf16, f32 = jnp.bfloat16, jnp.float32
     vmem, dma = pltpu.VMEM, pltpu.SemaphoreType.DMA
     here, there = pl.BlockSpec(memory_space=pltpu.VMEM), pl.BlockSpec(memory_space=pl.ANY)
     return pl.pallas_call(
-        expert_kernel,
-        out_shape=jax.ShapeDtypeStruct((own_rows, width), bf16),
-        in_specs=[here] * 5 + [there] * 6,
-        out_specs=here,
+        both_kernel,
+        out_shape=(
+            jax.ShapeDtypeStruct((tokens, head_dim), bf16),
+            jax.ShapeDtypeStruct((own_rows, width), bf16),
+        ),
+        in_specs=[here] * 8 + [there] * 6,
+        out_specs=(here, here),
         scratch_shapes=[
+            vmem((32, 2 * tokens + 16, head_dim), bf16),
+            vmem((2, 128, 128), f32),
             vmem((4, hidden, width), bf16),
             vmem((2, hidden, width), bf16),
             vmem((3, hidden, width), bf16),
@@ -625,6 +756,13 @@
             dma,
             dma,
             dma,
+            dma((8,)),
+            dma((9,)),
+            dma((8,)),
+            dma((9,)),
+            dma((16,)),
+            dma((16,)),
+            *attention_state(tokens, head_dim),
         ],
         compiler_params=pltpu.CompilerParams(
             collective_id=0, has_side_effects=True, vmem_limit_bytes=60 * 1024 * 1024
@@ -633,11 +771,14 @@
             flops=80_000_000_000, bytes_accessed=200_000_000, transcendentals=300_000
         ),
     )(
+        queries,
+        keys,
+        values,
+        bias_rows,
         moe_in,
         norm_gain[None, :],
-        route_ids,
         route_ids.T,
-        route_weights,
+        route_weights.T,
         gate_weight,
         up_weight,
         down_weight,
@@ -663,8 +804,11 @@
     shared_up,
     shared_down,
 ):
-    heads_out = stick_half(queries, keys, values, key_bias)
-    moe_out = expert_half(
+    return both_halves(
+        queries,
+        keys,
+        values,
+        key_bias,
         moe_in,
         norm_gain,
         route_ids,
@@ -676,7 +820,6 @@
         shared_up,
         shared_down,
     )
-    return (heads_out, moe_out)
 
 
 def solution(mesh):

time: 155 us -> 126 us (0.81)
  the two profiles are of different devices: /device:TPU:481 before, /device:TPU:129 now
where the time goes in v4:
time: 126 us
  Pallas kernels  122 us (97%)
  local copies, waits for them, and re-layouts  3.44 us (3%)
    pallas_call x1, Pallas kernels, both_halves(): pl.pallas_call(both_kernel, out_shape=(jax.ShapeDtypeStruct((tokens, head...  122 us
    unnamed x6, local copies, waits for them, and re-layouts  2.84 us

profile of v4, /device:TPU:129, one launch (start us, length us, event | category | flops | bytes accessed | tf_op | source)
XLA Modules:
  0.0 125.7 jit_solution(7925601949454953207)
XLA Ops:
  0.6 0.0 copy-start.1
  0.6 0.7 copy-done.1
  1.3 0.6 pad.4.bias_rows
  1.9 121.6 %shard_map.149 = (bf16[384,128]{1,0:T(8,128)(2,1)}, bf16[8,2048]{1,0:T(8,128)(2,1)}) custom-call(bf16[384,128]{1,0:T(8,128)(2,1)} %queries.1, bf16[384,128]{1,0:T(8,128)(2,1)} %keys.1, bf16[384,128]{1,0:T(8,128)(2,1)} %values.1, bf16[16,128]{1,0:T(8,128)(2,1)} %pad.4.bias_rows, bf16[8,2048]{1,0:T(8,128)(2,1)} %moe_in.1, f32[1,2048]{1,0:T(1,128)} %bitcast.5, ...), custom_call_target="tpu_custom_call" | custom-call | flops 80000000000 | bytes 200000000 | tf_op jit(solution)/shard_map/pallas_call | solution.py:717
  123.5 0.0 copy-start
  123.5 1.5 %copy.18 = bf16[384,128]{1,0:T(8,128)(2,1)} copy(bf16[384,128]{1,0:T(8,128)(2,1)} %get-tuple-element.4) | data formatting | bytes 196608
  125.1 0.0 copy-done
  125.1 0.6 copy.19
  (1 shorter events, 0.0 us)
Async XLA Ops:
  0.6 0.7 copy-start.1
  123.5 1.6 %copy-start = (bf16[8,2048]{1,0:T(8,128)(2,1)S(1)}, bf16[8,2048]{1,0:T(8,128)(2,1)}, u32[]{:S(2)}) copy-start(bf16[8,2048]{1,0:T(8,128)(2,1)} %get-tuple-element.5) | copy-start | bytes 98308

commit v5 on v4

--- a/solution.py
+++ b/solution.py
@@ -245,6 +245,81 @@
 
     pl.semaphore_wait(barrier, ep_count + tp_count - 2)
 
+    chips = ep_count // 2
+    z, core = e // 2, lax.rem(e, 2)
+    partner = e + 1 - 2 * core
+    most_up, most_down = chips // 2, chips // 2 - 1
+
+    def kv_copy(chip, target, send_sem, recv_sem):
+        ref = kv.at[chip * 2 + core]
+        return pltpu.make_async_remote_copy(
+            ref, ref, send_sem, recv_sem, device_id={"ep": target}, device_id_type=MESH
+        )
+
+    def chip_at(step):
+        return lax.rem(z + step + chips, chips)
+
+    def up_copy(n):
+        return kv_copy(
+            chip_at(-n), chip_at(1) * 2 + core, up_send.at[n], up_recv.at[n + 1]
+        )
+
+    def down_copy(n):
+        return kv_copy(
+            chip_at(n), chip_at(-1) * 2 + core, down_send.at[n], down_recv.at[n + 1]
+        )
+
+    def pair_copy(chip):
+        return kv_copy(chip, partner, pair_send.at[chip], pair_recv.at[chip])
+
+    def goes_up(n):
+        return (z - n >= 0) & (z < chips - 1)
+
+    def goes_down(n):
+        return chip_at(n) < most_down
+
+    def kv_service(n):
+        @pl.when(z >= n)
+        def _():
+            up_copy(n - 1).wait_recv()
+            pair_copy(z - n).start()
+
+        if n < most_up:
+
+            @pl.when(goes_up(n))
+            def _():
+                up_copy(n).start()
+
+        if n <= most_down:
+
+            @pl.when(goes_down(n))
+            def _():
+                down_copy(n - 1).wait_recv()
+
+                @pl.when(chip_at(n) < z)
+                def _():
+                    pair_copy(chip_at(n)).start()
+
+                if n < most_down:
+                    down_copy(n).start()
+
+    def attend(first, last):
+        def pair(n, carry):
+            @pl.when(z >= n)
+            def _():
+                pair_wait(z - n)
+                for extra in range(2):
+                    attention_step(state, queries, kv, e, 2 * n - 1 + core + extra)
+
+            return carry
+
+        lax.fori_loop(first, last + 1, pair, 0)
+
+    def pair_wait(chip):
+        ref = kv.at[chip * 2 + 1 - core]
+        pltpu.make_async_copy(ref, ref, pair_recv.at[chip]).wait()
+
+
     def send_pre(k, carry):
         other, device = tp_peer(k)
         pltpu.make_async_remote_copy(
@@ -260,7 +335,19 @@
         return carry
 
     lax.fori_loop(1, tp_count, send_pre, 0)
-    lax.fori_loop(1, tp_count, send_mix, 0)
+
+    @pl.when(core == 0)
+    def _():
+        pair_copy(z).start()
+
+    @pl.when(goes_up(0))
+    def _():
+        up_copy(0).start()
+
+    @pl.when(goes_down(0))
+    def _():
+        down_copy(0).start()
+
 
     across = ids_across[...]
     expert_id = lax.broadcasted_iota(jnp.int32, (64, 128), 0)
@@ -300,93 +387,18 @@
         return carry
 
     lax.fori_loop(1, ep_count, send_go, 0)
+    lax.fori_loop(1, tp_count, send_mix, 0)
     pooled[t, at_e, :] = outgoing[at_e, :]
-
-    chips = ep_count // 2
-    z, core = e // 2, lax.rem(e, 2)
-    partner = e + 1 - 2 * core
-    most_up, most_down = chips // 2, chips // 2 - 1
-
-    def kv_copy(chip, target, send_sem, recv_sem):
-        ref = kv.at[chip * 2 + core]
-        return pltpu.make_async_remote_copy(
-            ref, ref, send_sem, recv_sem, device_id={"ep": target}, device_id_type=MESH
-        )
-
-    def chip_at(step):
-        return lax.rem(z + step + chips, chips)
-
-    def up_copy(n):
-        return kv_copy(
-            chip_at(-n), chip_at(1) * 2 + core, up_send.at[n], up_recv.at[n + 1]
-        )
-
-    def down_copy(n):
-        return kv_copy(
-            chip_at(n), chip_at(-1) * 2 + core, down_send.at[n], down_recv.at[n + 1]
-        )
-
-    def pair_copy(chip):
-        return kv_copy(chip, partner, pair_send.at[chip], pair_recv.at[chip])
-
-    def goes_up(n):
-        return (z - n >= 0) & (z < chips - 1)
-
-    def goes_down(n):
-        return chip_at(n) < most_down
-
-    @pl.when(core == 0)
+    kv_service(1)
+    k_block, _, own_bias = attention_parts(kv, e, tokens)
+    attention_score_block(state, queries, k_block, own_bias, True)
+
+    @pl.when(core == 1)
     def _():
-        pair_copy(z).start()
-
-    @pl.when(goes_up(0))
-    def _():
-        up_copy(0).start()
-
-    @pl.when(goes_down(0))
-    def _():
-        down_copy(0).start()
-
-    def kv_service(n):
-        @pl.when(z >= n)
-        def _():
-            up_copy(n - 1).wait_recv()
-            pair_copy(z - n).start()
-
-        if n < most_up:
-
-            @pl.when(goes_up(n))
-            def _():
-                up_copy(n).start()
-
-        if n <= most_down:
-
-            @pl.when(goes_down(n))
-            def _():
-                down_copy(n - 1).wait_recv()
-
-                @pl.when(chip_at(n) < z)
-                def _():
-                    pair_copy(chip_at(n)).start()
-
-                if n < most_down:
-                    down_copy(n).start()
-
-    def attend(first, last):
-        def pair(n, carry):
-            @pl.when(z >= n)
-            def _():
-                pair_wait(z - n)
-                for extra in range(2):
-                    attention_step(state, queries, kv, e, 2 * n - 1 + core + extra)
-
-            return carry
-
-        lax.fori_loop(first, last + 1, pair, 0)
-
-    def pair_wait(chip):
-        ref = kv.at[chip * 2 + 1 - core]
-        pltpu.make_async_copy(ref, ref, pair_recv.at[chip]).wait()
+        pair_wait(z)
+        attention_step(state, queries, kv, e, 1)
+
+    attend(1, 1)
 
     pltpu.make_async_copy(
         mixes.at[pl.ds(0, tp_count - 1)], mixes.at[pl.ds(0, tp_count - 1)], mix_recv
@@ -405,9 +417,6 @@
                 jnp.bfloat16
             )
 
-    k_block, _, own_bias = attention_parts(kv, e, tokens)
-    attention_score_block(state, queries, k_block, own_bias, True)
-
     pltpu.make_async_copy(
         pooled.at[t, pl.ds(0, 992)], pooled.at[t, pl.ds(0, 992)], go_recv
     ).wait()
@@ -462,6 +471,7 @@
         ag_copy(q, -d, 0, True, d).start()
         ag_copy(q, -d, 0, False, 1).start()
         ag_copy(q, -d, 0, False, 3).start()
+    kv_service(2)
     for q in quarters:
         d = axes(q)[2]
         ag_wait(q, d, 0)
@@ -475,21 +485,19 @@
         ag_wait(q, 2, 0)
         ag_copy(q, 2, 0, False, 1).start()
         ag_copy(q, 2, 0, False, 3).start()
-    kv_service(1)
-
-    @pl.when(core == 1)
-    def _():
-        pair_wait(z)
-        attention_step(state, queries, kv, e, 1)
-
+        if q == 1:
+            kv_service(3)
     for hop in range(3):
         for q in quarters:
             d = axes(q)[2]
             df = (-d, d, 2)[hop]
             ag_wait(q, df, -d)
             ag_copy(q, df, -d, False, d).start()
-        if hop > 0:
-            kv_service(hop + 1)
+            if hop == 1 and q == 1:
+                kv_service(4)
+    attend(2, 2)
+    kv_service(5)
+    attend(3, 3)
 
     for load in loads:
         load.wait()
@@ -559,11 +567,10 @@
             slot = (df % 4) * 3
             rs_copy(q, block(partial, q, df, 2), slot, False, d).start()
             rs_copy(q, block(partial, q, df, -d), slot + 1, False, -d).start()
-
-    kv_service(4)
-    attend(1, 3)
-    kv_service(5)
-    attend(4, 4)
+        if q == 1:
+            kv_service(6)
+
+    attend(4, 5)
     rows_of = lambda q: slice(q * quarter, (q + 1) * quarter)
     for turn in range(4):
         for q in quarters:
@@ -573,9 +580,9 @@
             where, total = plus(q, df, d, df * 3)
             partial[where, rows_of(q), :] = total.astype(jnp.bfloat16)
             rs_copy(q, block(partial, q, df, d), df * 3 + 2, False, d).start()
-        if turn < 3:
-            kv_service(turn + 6)
-        attend(turn + 5, turn + 5)
+        if turn < 2:
+            kv_service(turn + 7)
+        attend(turn + 6, turn + 6)
     for turn in range(4):
         for q in quarters:
             d = axes(q)[2]
@@ -595,7 +602,7 @@
             elif turn == 2:
                 rs_copy(q, block(partial, q, df, 0), 14, True, d).start()
         if turn < 3:
-            attend(turn + 9, turn + 9)
+            attend(turn + 10, turn + 10)
 
     for q in quarters:
         rs_wait(q, 13)
@@ -621,7 +628,7 @@
 
         lax.fori_loop(q * 9, min(ep_count, (q + 1) * 9), send_back, 0)
     returned[at_e, :] = result[at_e, :]
-    attend(12, chips - 1)
+    attend(13, chips - 1)
     for extra in range(2):
         attention_step(state, queries, kv, e, e + 1 + extra)
     attention_end(state, heads)

time: 126 us -> 120 us (0.952)
  the two profiles are of different devices: /device:TPU:129 before, /device:TPU:96 now
where the time goes in v5:
time: 120 us
  Pallas kernels  116 us (97%)
  local copies, waits for them, and re-layouts  3.44 us (3%)
    pallas_call x1, Pallas kernels, both_halves(): pl.pallas_call(both_kernel, out_shape=(jax.ShapeDtypeStruct((tokens, head...  116 us
    unnamed x6, local copies, waits for them, and re-layouts  2.84 us

profile of v5, /device:TPU:96, one launch (start us, length us, event | category | flops | bytes accessed | tf_op | source)
XLA Modules:
  0.0 119.7 jit_solution(4198950415492967016)
XLA Ops:
  0.6 0.0 copy-start.1
  0.6 0.7 copy-done.1
  1.3 0.6 pad.4.bias_rows
  1.9 115.6 %shard_map.149 = (bf16[384,128]{1,0:T(8,128)(2,1)}, bf16[8,2048]{1,0:T(8,128)(2,1)}) custom-call(bf16[384,128]{1,0:T(8,128)(2,1)} %queries.1, bf16[384,128]{1,0:T(8,128)(2,1)} %keys.1, bf16[384,128]{1,0:T(8,128)(2,1)} %values.1, bf16[16,128]{1,0:T(8,128)(2,1)} %pad.4.bias_rows, bf16[8,2048]{1,0:T(8,128)(2,1)} %moe_in.1, f32[1,2048]{1,0:T(1,128)} %bitcast.5, ...), custom_call_target="tpu_custom_call" | custom-call | flops 80000000000 | bytes 200000000 | tf_op jit(solution)/shard_map/pallas_call | solution.py:724
  117.5 0.0 copy-start
  117.5 1.5 %copy.18 = bf16[384,128]{1,0:T(8,128)(2,1)} copy(bf16[384,128]{1,0:T(8,128)(2,1)} %get-tuple-element.4) | data formatting | bytes 196608
  119.1 0.0 copy-done
  119.1 0.6 copy.19
  (1 shorter events, 0.0 us)
Async XLA Ops:
  0.6 0.7 copy-start.1
  117.5 1.6 %copy-start = (bf16[8,2048]{1,0:T(8,128)(2,1)S(1)}, bf16[8,2048]{1,0:T(8,128)(2,1)}, u32[]{:S(2)}) copy-start(bf16[8,2048]{1,0:T(8,128)(2,1)} %get-tuple-element.5) | copy-start | bytes 98308

commit v6 on v5

--- a/solution.py
+++ b/solution.py
@@ -571,6 +571,7 @@
             kv_service(6)
 
     attend(4, 5)
+    kv_service(7)
     rows_of = lambda q: slice(q * quarter, (q + 1) * quarter)
     for turn in range(4):
         for q in quarters:
@@ -580,9 +581,9 @@
             where, total = plus(q, df, d, df * 3)
             partial[where, rows_of(q), :] = total.astype(jnp.bfloat16)
             rs_copy(q, block(partial, q, df, d), df * 3 + 2, False, d).start()
-        if turn < 2:
-            kv_service(turn + 7)
         attend(turn + 6, turn + 6)
+        if turn == 1:
+            kv_service(8)
     for turn in range(4):
         for q in quarters:
             d = axes(q)[2]

time: 120 us -> 118 us (0.983)
  the two profiles are of different devices: /device:TPU:96 before, /device:TPU:65 now
where the time goes in v6:
time: 118 us
  Pallas kernels  114 us (97%)
  local copies, waits for them, and re-layouts  3.44 us (3%)
    pallas_call x1, Pallas kernels, both_halves(): pl.pallas_call(both_kernel, out_shape=(jax.ShapeDtypeStruct((tokens, head...  114 us
    unnamed x6, local copies, waits for them, and re-layouts  2.84 us

profile of v6, /device:TPU:65, one launch (start us, length us, event | category | flops | bytes accessed | tf_op | source)
XLA Modules:
  0.0 117.7 jit_solution(17382807351747863594)
XLA Ops:
  0.6 0.0 copy-start.1
  0.6 0.7 copy-done.1
  1.3 0.6 pad.4.bias_rows
  1.9 113.6 %shard_map.149 = (bf16[384,128]{1,0:T(8,128)(2,1)}, bf16[8,2048]{1,0:T(8,128)(2,1)}) custom-call(bf16[384,128]{1,0:T(8,128)(2,1)} %queries.1, bf16[384,128]{1,0:T(8,128)(2,1)} %keys.1, bf16[384,128]{1,0:T(8,128)(2,1)} %values.1, bf16[16,128]{1,0:T(8,128)(2,1)} %pad.4.bias_rows, bf16[8,2048]{1,0:T(8,128)(2,1)} %moe_in.1, f32[1,2048]{1,0:T(1,128)} %bitcast.5, ...), custom_call_target="tpu_custom_call" | custom-call | flops 80000000000 | bytes 200000000 | tf_op jit(solution)/shard_map/pallas_call | solution.py:725
  115.5 0.0 copy-start
  115.5 1.5 %copy.18 = bf16[384,128]{1,0:T(8,128)(2,1)} copy(bf16[384,128]{1,0:T(8,128)(2,1)} %get-tuple-element.4) | data formatting | bytes 196608
  117.1 0.0 copy-done
  117.1 0.6 copy.19
  (1 shorter events, 0.0 us)
Async XLA Ops:
  0.6 0.7 copy-start.1
  115.5 1.6 %copy-start = (bf16[8,2048]{1,0:T(8,128)(2,1)S(1)}, bf16[8,2048]{1,0:T(8,128)(2,1)}, u32[]{:S(2)}) copy-start(bf16[8,2048]{1,0:T(8,128)(2,1)} %get-tuple-element.5) | copy-start | bytes 98308
